TPU v7x, 256 devices: a 4x2x16 block of a 4x16x16 slice. The times are simulated.
256 devices in a mesh: grp: 2 (over y), sp: 32 (over z, core), tp: 4 (over x).
Axes of the slice: x: 4, y: 2, z: 16, core: 2. Of those that a mesh axis runs over, the one named last changes fastest.
The devices are a block of a 4x16x16 slice.
Arguments:
- conv_value: bfloat16 [32768, 1024], P(('grp', 'sp'), 'tp'), parts along dimension 0, may hold values from -6 to 6
- conv_gate: bfloat16 [32768, 1024], P(('grp', 'sp'), 'tp'), parts along dimension 0, may hold values from -6 to 6
- kernel: bfloat16 [31, 1024], P(None, 'tp'), may hold values from -4 to 4
- conv_bias: float32 [1024], P('tp'), may hold values from -3 to 3
- ln_gain: float32 [1024], P('tp'), may hold values from 0.1 to 1.9
- ln_bias: float32 [1024], P('tp'), may hold values from -3 to 3
- out_gain: float32 [1024], P('tp'), may hold values from 0.1 to 1.9
- out_weight: bfloat16 [1024, 2048], replicated, may hold values from -0.1875 to 0.1875
- residual: bfloat16 [32768, 2048], P(('grp', 'sp', 'tp')), parts along dimension 0, may hold values from -6 to 6
- moe_gain: float32 [2048], replicated, may hold values from 0.1 to 1.9
- expert_ids: int32 [32768, 2], P(('grp', 'sp', 'tp')), parts along dimension 0, may hold values from 0 to 127, as said below
- expert_weights: float32 [32768, 2], P(('grp', 'sp', 'tp')), parts along dimension 0, may hold values from 0.1 to 0.7
- w_gate: bfloat16 [128, 2048, 512], P(('sp', 'tp')), may hold values from -0.125 to 0.125
- w_up: bfloat16 [128, 2048, 512], P(('sp', 'tp')), may hold values from -0.125 to 0.125
- w_down: bfloat16 [128, 512, 2048], P(('sp', 'tp')), may hold values from -0.25 to 0.25
Outputs:
- layer_out: bfloat16 [32768, 2048], P(('grp', 'sp', 'tp')), parts along dimension 0
There are 2 independent parts, one for each index of `grp`. A program takes and returns all parts, laid end to end along the dimension named above; an argument that names none is the same for every part. Nothing has to cross between parts.
Inputs may be any that keep to these rules, and one draw needn't show every extreme that they name: `expert_ids`: each row names two different experts of one group (group = expert number // 32). Among the 128 rows of one device (aligned blocks of 128 rows) no expert is named more than 4 times, and in every such block some expert is named exactly 4 times.
All inputs are finite; a program needn't handle non-finite values.
Results may differ from a plain program's by a relative error of at most 0.0095.
Values may be sent and summed in bfloat16 or wider, within the bound.
A program may use at most 64 MiB of HBM per device.

v0:
```python
import jax
import jax.numpy as jnp
from jax import lax
from jax.sharding import PartitionSpec as P

EPSILON = 1e-06


def passed_along(block, axis, distance):
    devices = range(lax.axis_size(axis))
    route = [(i - distance, i) for i in devices if i - distance in devices]
    return lax.ppermute(block, axis, route)


def copy_for_each(shard, axis):
    size = lax.axis_size(axis)
    return lax.all_to_all(
        jnp.broadcast_to(shard[None], (size, *shard.shape)), axis, 0, 0, tiled=True
    )


def of_everyone(shard, axis):
    return copy_for_each(shard, axis).sum(axis=0)


def together(arrays, axis):
    ends = [0]
    for a in arrays:
        ends.append(ends[-1] + a.size)
    subtotal = of_everyone(jnp.concatenate([a.ravel() for a in arrays]), axis)
    return tuple((subtotal[b:e].reshape(a.shape) for a, b, e in zip(arrays, ends, ends[1:])))


def per_device(
    conv_value,
    conv_gate,
    kernel,
    conv_bias,
    ln_gain,
    ln_bias,
    out_gain,
    out_weight,
    residual,
    moe_gain,
    expert_ids,
    expert_weights,
    w_gate,
    w_up,
    w_down,
):
    tok_rows, channels = conv_value.shape
    reach_rows = kernel.shape[0] - 1
    full_channels = channels * lax.axis_size("tp")
    gated = (conv_value.astype(jnp.float32) * jax.nn.sigmoid(conv_gate.astype(jnp.float32))).astype(
        jnp.bfloat16
    )
    before = passed_along(gated[tok_rows - reach_rows :], "sp", 1)
    padded = jnp.concatenate([before, gated], axis=0)
    convolved = jnp.zeros((tok_rows, channels), jnp.float32) + conv_bias
    for offset in range(reach_rows + 1):
        convolved = convolved + padded[offset : offset + tok_rows].astype(jnp.float32) * kernel[
            offset
        ].astype(jnp.float32)
    totals = together((jnp.sum(convolved, axis=1), jnp.sum(convolved * convolved, axis=1)), "tp")
    average = (totals[0] / full_channels)[:, None]
    spread = (totals[1] / full_channels)[:, None] - average * average
    swished = jax.nn.silu((convolved - average) * lax.rsqrt(spread + EPSILON) * ln_gain + ln_bias)
    energy = of_everyone(jnp.sum(swished * swished, axis=1), "tp")
    branch = (swished * lax.rsqrt(energy / full_channels + EPSILON)[:, None] * out_gain).astype(
        jnp.bfloat16
    )
    row_count = tok_rows // lax.axis_size("tp")
    regrouped = lax.all_to_all(branch, "tp", split_axis=0, concat_axis=1, tiled=True)
    projected = jnp.dot(regrouped, out_weight, preferred_element_type=jnp.float32)
    hidden = (residual.astype(jnp.float32) + projected).astype(jnp.bfloat16)
    widened = hidden.astype(jnp.float32)
    normed = (
        widened * lax.rsqrt(jnp.mean(widened * widened, axis=1, keepdims=True) + EPSILON) * moe_gain
    ).astype(jnp.bfloat16)
    width = normed.shape[1]
    experts = lax.axis_size("sp") * lax.axis_size("tp")
    capacity = 2 * row_count // min(row_count, experts // 2)
    flat_ids = expert_ids.reshape(-1)
    onehot = (flat_ids[:, None] == jnp.arange(experts, dtype=jnp.int32)[None, :]).astype(jnp.int32)
    slot_rank = jnp.sum((jnp.cumsum(onehot, axis=0) - 1) * onehot, axis=1)
    position = flat_ids * capacity + slot_rank
    outgoing = (
        jnp.zeros((experts * capacity, width), jnp.bfloat16)
        .at[position]
        .set(jnp.repeat(normed, 2, axis=0))
    )
    outgoing = outgoing.reshape(experts, capacity, width)
    arriving = lax.all_to_all(outgoing, ("sp", "tp"), split_axis=0, concat_axis=0, tiled=True)
    flattened = arriving.reshape(-1, width)
    gate_part = jnp.dot(flattened, w_gate[0], preferred_element_type=jnp.float32)
    up_part = jnp.dot(flattened, w_up[0], preferred_element_type=jnp.float32)
    active = (jax.nn.silu(gate_part) * up_part).astype(jnp.bfloat16)
    result = jnp.dot(active, w_down[0], preferred_element_type=jnp.float32).astype(jnp.bfloat16)
    produced = result.reshape(arriving.shape)
    returned = lax.all_to_all(produced, ("sp", "tp"), split_axis=0, concat_axis=0, tiled=True)
    returned = returned.reshape(experts * capacity, width)
    picked = returned[position].reshape(row_count, 2, width)
    combined = jnp.sum(picked.astype(jnp.float32) * expert_weights[:, :, None], axis=1)
    return (widened + combined).astype(jnp.bfloat16)


def solution(mesh):
    in_specs = (
        P(("grp", "sp"), "tp"),
        P(("grp", "sp"), "tp"),
        P(None, "tp"),
        P("tp"),
        P("tp"),
        P("tp"),
        P("tp"),
        P(),
        P(("grp", "sp", "tp"), None),
        P(),
        P(("grp", "sp", "tp"), None),
        P(("grp", "sp", "tp"), None),
        P(("sp", "tp"), None, None),
        P(("sp", "tp"), None, None),
        P(("sp", "tp"), None, None),
    )
    out_specs = P(("grp", "sp", "tp"), None)
    return jax.shard_map(
        per_device, mesh=mesh, in_specs=in_specs, out_specs=out_specs, check_vma=False
    )
```

profile of v0, /device:TPU:40, one launch (start us, length us, event | category | flops | bytes accessed | tf_op | source)
XLA Modules:
  0.0 327.8 jit_solution(4955386901156573632)
XLA Ops:
  1.4 1.8 collective-permute-start
  6.6 3.2 fusion.52
  10.5 4.6 %all-to-all-start = ((f32[4,1,1024]{2,1,0:T(1,128)}), f32[4,1,1024]{2,1,0:T(1,128)S(1)}, u32[]{:S(2)}, u32[]{:S(2)}) async-start(f32[4,1,1024]{2,1,0:T(1,128)} %broadcast_in_dim.8), calls=%async_computation | async-start | bytes 32768 | tf_op jit(solution)/shard_map/all_to_all | solution.py:17
  15.2 5.2 %all-to-all-done = f32[4,1,1024]{2,1,0:T(1,128)S(1)} async-done(((f32[4,1,1024]{2,1,0:T(1,128)}), f32[4,1,1024]{2,1,0:T(1,128)S(1)}, u32[]{:S(2)}, u32[]{:S(2)}) %all-to-all-start) | async-done | bytes 16416 | tf_op jit(solution)/shard_map/all_to_all | solution.py:17
  21.5 3.3 %all-to-all-start.1 = ((f32[4,1,512]{2,1,0:T(1,128)}), f32[4,1,512]{2,1,0:T(1,128)S(1)}, u32[]{:S(2)}, u32[]{:S(2)}) async-start(f32[4,1,512]{2,1,0:T(1,128)} %broadcast_in_dim.9), calls=%async_computation.1 | async-start | bytes 16384 | tf_op jit(solution)/shard_map/all_to_all | solution.py:17
  25.3 4.8 %all-to-all-done.1 = f32[4,1,512]{2,1,0:T(1,128)S(1)} async-done(((f32[4,1,512]{2,1,0:T(1,128)}), f32[4,1,512]{2,1,0:T(1,128)S(1)}, u32[]{:S(2)}, u32[]{:S(2)}) %all-to-all-start.1) | async-done | bytes 8224 | tf_op jit(solution)/shard_map/all_to_all | solution.py:17
  30.9 3.5 %all-to-all-start.2 = ((bf16[4,128,256]{2,1,0:T(8,128)(2,1)}), bf16[4,128,256]{2,1,0:T(8,128)(2,1)S(1)}, u32[]{:S(2)}, u32[]{:S(2)}) async-start(bf16[4,128,256]{2,1,0:T(8,128)(2,1)} %bitcast.31), calls=%async_computation.2 | async-start | bytes 524288 | tf_op jit(solution)/shard_map/all_to_all | solution.py:73
  34.4 7.4 %all-to-all-done.2 = bf16[4,128,256]{2,1,0:T(8,128)(2,1)S(1)} async-done(((bf16[4,128,256]{2,1,0:T(8,128)(2,1)}), bf16[4,128,256]{2,1,0:T(8,128)(2,1)S(1)}, u32[]{:S(2)}, u32[]{:S(2)}) %all-to-all-start.2) | async-done | bytes 262176 | tf_op jit(solution)/shard_map/all_to_all | solution.py:73
  42.0 3.1 multiply_reduce_fusion.1
  45.4 1.6 broadcast_in_dim.11
  47.0 2.3 reshape.156
  49.2 4.4 %scatter_custom_fusion = bf16[512,2048]{1,0:T(8,128)(2,1)} fusion(s32[256]{0:T(256)S(1)} %bitcast.97, bf16[256,2048]{1,0:T(8,128)(2,1)} %reshape.156, bf16[]{:T(256)} %constant.15.clone.1), kind=kCustom, calls=%fused_computation.46 | custom fusion | bytes 2097664 | tf_op jit(solution)/shard_map/scatter | solution.py:90
  53.7 4.1 %reshape.108 = bf16[128,4,2048]{2,1,0:T(4,128)(2,1)} reshape(bf16[512,2048]{1,0:T(8,128)(2,1)} %scatter_custom_fusion) | data formatting | bytes 4194304 | tf_op jit(solution)/shard_map/reshape | solution.py:92
  57.8 125.1 %all_to_all.41 = bf16[128,4,2048]{2,1,0:T(4,128)(2,1)} all-to-all(bf16[128,4,2048]{2,1,0:T(4,128)(2,1)} %reshape.108), channel_id=1, replica_groups=mesh['grp'=2,'sp'=32,'tp'=4] {'sp','tp'}, dimensions={0} | all-to-all | bytes 4194304 | tf_op jit(solution)/shard_map/all_to_all | solution.py:93
  182.9 4.0 %reshape.109 = bf16[512,2048]{1,0:T(8,128)(2,1)} reshape(bf16[128,4,2048]{2,1,0:T(4,128)(2,1)} %all_to_all.41) | data formatting | bytes 4194304 | tf_op jit(solution)/shard_map/reshape | solution.py:94
  186.8 4.4 %fusion.5 = f32[512,512]{1,0:T(8,128)} fusion(bf16[512,2048]{1,0:T(8,128)(2,1)} %reshape.109, bf16[1,2048,512]{2,1,0:T(8,128)(2,1)} %param.27), kind=kOutput, calls=%fused_computation.38 | convolution fusion | flops 1073741824 | bytes 5242880 | tf_op jit(solution)/shard_map/dot_general | solution.py:95
  191.3 6.2 %convolution_convert_fusion = bf16[512,2048]{1,0:T(8,128)(2,1)} fusion(bf16[1,512,2048]{2,1,0:T(8,128)(2,1)S(1)} %copy-done, bf16[512,2048]{1,0:T(8,128)(2,1)} %reshape.109, bf16[1,2048,512]{2,1,0:T(8,128)(2,1)} %param.28, f32[512,512]{1,0:T(8,128)} %fusion.5), kind=kOutput, calls=%fused_computation.31 | convolution fusion | flops 2150105088 | bytes 9437184 | tf_op jit(solution)/shard_map/dot_general | solution.py:98
  197.5 4.1 %reshape.110 = bf16[128,4,2048]{2,1,0:T(4,128)(2,1)} reshape(bf16[512,2048]{1,0:T(8,128)(2,1)} %convolution_convert_fusion) | data formatting | bytes 4194304 | tf_op jit(solution)/shard_map/reshape | solution.py:99
  201.6 12.4 %all-to-all-start.4 = ((bf16[128,4,2048]{2,1,0:T(4,128)(2,1)}), bf16[128,4,2048]{2,1,0:T(4,128)(2,1)}, u32[]{:S(2)}, u32[]{:S(2)}) async-start(bf16[128,4,2048]{2,1,0:T(4,128)(2,1)} %reshape.110), calls=%async_computation.4 | async-start | bytes 4194304 | tf_op jit(solution)/shard_map/all_to_all | solution.py:100
  214.2 95.4 %all-to-all-done.4 = bf16[128,4,2048]{2,1,0:T(4,128)(2,1)} async-done(((bf16[128,4,2048]{2,1,0:T(4,128)(2,1)}), bf16[128,4,2048]{2,1,0:T(4,128)(2,1)}, u32[]{:S(2)}, u32[]{:S(2)}) %all-to-all-start.4) | async-done | bytes 2097184 | tf_op jit(solution)/shard_map/all_to_all | solution.py:100
  309.5 4.0 %reshape.111 = bf16[512,2048]{1,0:T(8,128)(2,1)} reshape(bf16[128,4,2048]{2,1,0:T(4,128)(2,1)} %all-to-all-done.4) | data formatting | bytes 4194304 | tf_op jit(solution)/shard_map/reshape | solution.py:101
  313.5 5.2 %gather_fusion = bf16[256,2048]{1,0:T(8,128)(2,1)} fusion(bf16[512,2048]{1,0:T(8,128)(2,1)} %reshape.111, s32[1024]{0:T(1024)S(1)} %pad_clamp_fusion), kind=kCustom, calls=%fused_computation | custom fusion | bytes 2098176 | tf_op jit(solution)/shard_map/gather | solution.py:102
  318.7 3.4 %reshape.143 = f32[128,2,2048]{2,1,0:T(2,128)} reshape(bf16[256,2048]{1,0:T(8,128)(2,1)} %gather_fusion) | data formatting | bytes 3145728 | tf_op jit(solution)/shard_map/convert_element_type | solution.py:103
  322.1 4.8 %multiply_reduce_fusion = f32[128,2048]{1,0:T(8,128)S(1)} fusion(f32[128,2,2048]{2,1,0:T(2,128)} %reshape.143, f32[128,2]{1,0:T(8,128)S(1)} %copy.45), kind=kLoop, calls=%fused_computation.40 | loop fusion | flops 786432 | bytes 3146752 | tf_op jit(solution)/shard_map/reduce_sum | solution.py:103
  (49 shorter events, 9.2 us)
Async XLA Ops:
  0.0 191.3 %copy-start = (bf16[1,512,2048]{2,1,0:T(8,128)(2,1)S(1)}, bf16[1,512,2048]{2,1,0:T(8,128)(2,1)}, u32[]{:S(2)}) copy-start(bf16[1,512,2048]{2,1,0:T(8,128)(2,1)} %param.29) | copy-start | bytes 6291460
  0.0 15.1 %copy-start.2 = (s32[128,2]{0,1:T(2,128)S(1)}, s32[128,2]{0,1:T(2,128)}, u32[]{:S(2)}) copy-start(s32[128,2]{0,1:T(2,128)} %param.25) | copy-start | bytes 3076
  0.0 20.5 %copy-start.6 = (f32[256]{0:T(256)S(1)}, f32[256]{0:T(256)}, u32[]{:S(2)}) copy-start(f32[256]{0:T(256)} %param.19) | copy-start | bytes 3076
  0.0 20.5 %copy-start.5 = (f32[256]{0:T(256)S(1)}, f32[256]{0:T(256)}, u32[]{:S(2)}) copy-start(f32[256]{0:T(256)} %param.20) | copy-start | bytes 3076
  0.0 30.1 %copy-start.3 = (f32[256]{0:T(256)S(1)}, f32[256]{0:T(256)}, u32[]{:S(2)}) copy-start(f32[256]{0:T(256)} %param.21) | copy-start | bytes 3076
  1.4 5.3 %collective-permute-start = (bf16[30,256]{1,0:T(8,128)(2,1)S(1)}, bf16[30,256]{1,0:T(8,128)(2,1)S(1)}, u32[]{:S(2)}, u32[]{:S(2)}) collective-permute-start(bf16[30,256]{1,0:T(8,128)(2,1)S(1)} %slice.266), channel_id=1, source_target_pairs={{0,4},{4,8},{8,12},{12,16},{16,20},{20,24},{24,28},{28,32},{32,36}... | collective-permute-start | bytes 46088 | tf_op jit(solution)/shard_map/ppermute | solution.py:12
  10.5 9.9 %all-to-all-start = ((f32[4,1,1024]{2,1,0:T(1,128)}), f32[4,1,1024]{2,1,0:T(1,128)S(1)}, u32[]{:S(2)}, u32[]{:S(2)}) async-start(f32[4,1,1024]{2,1,0:T(1,128)} %broadcast_in_dim.8), calls=%async_computation | async-start | bytes 32768 | tf_op jit(solution)/shard_map/all_to_all | solution.py:17
  21.5 8.6 %all-to-all-start.1 = ((f32[4,1,512]{2,1,0:T(1,128)}), f32[4,1,512]{2,1,0:T(1,128)S(1)}, u32[]{:S(2)}, u32[]{:S(2)}) async-start(f32[4,1,512]{2,1,0:T(1,128)} %broadcast_in_dim.9), calls=%async_computation.1 | async-start | bytes 16384 | tf_op jit(solution)/shard_map/all_to_all | solution.py:17
  30.9 10.9 %all-to-all-start.2 = ((bf16[4,128,256]{2,1,0:T(8,128)(2,1)}), bf16[4,128,256]{2,1,0:T(8,128)(2,1)S(1)}, u32[]{:S(2)}, u32[]{:S(2)}) async-start(bf16[4,128,256]{2,1,0:T(8,128)(2,1)} %bitcast.31), calls=%async_computation.2 | async-start | bytes 524288 | tf_op jit(solution)/shard_map/all_to_all | solution.py:73
  42.0 3.2 copy-start.1
  201.6 12.4 %copy-start.4 = (f32[128,2]{0,1:T(2,128)S(1)}, f32[128,2]{0,1:T(2,128)}, u32[]{:S(2)}) copy-start(f32[128,2]{0,1:T(2,128)} %param.26) | copy-start | bytes 3076
  201.6 107.9 %all-to-all-start.4 = ((bf16[128,4,2048]{2,1,0:T(4,128)(2,1)}), bf16[128,4,2048]{2,1,0:T(4,128)(2,1)}, u32[]{:S(2)}, u32[]{:S(2)}) async-start(bf16[128,4,2048]{2,1,0:T(4,128)(2,1)} %reshape.110), calls=%async_computation.4 | async-start | bytes 4194304 | tf_op jit(solution)/shard_map/all_to_all | solution.py:100
where the time goes:
time: 330 us; the launch traced here: 328 us
  blocking collectives  125 us (38%)
  waiting for transfers between devices  113 us (34%)
  local copies, waits for them, and re-layouts  36 us (11%)
  starting transfers between devices  25.7 us (8%)
  other arithmetic  14.3 us (4%)
  matrix products  13.8 us (4%)
    all_to_all x1, blocking collectives, per_device(): lax.all_to_all(outgoing, ('sp', 'tp'), split_axis=0, concat_axis=0, tiled...  125 us
    all_to_all x1, waiting for transfers between devices, per_device(): lax.all_to_all(produced, ('sp', 'tp'), split_axis=0, concat_axis=0, tiled...  95.4 us
    all_to_all x1, starting transfers between devices, per_device(): lax.all_to_all(produced, ('sp', 'tp'), split_axis=0, concat_axis=0, tiled...  12.4 us
    all_to_all x2, waiting for transfers between devices, copy_for_each(): lax.all_to_all(jnp.broadcast_to(shard[None], (size, *shard.shape)), axis,...  9.98 us
    all_to_all x2, starting transfers between devices, copy_for_each(): lax.all_to_all(jnp.broadcast_to(shard[None], (size, *shard.shape)), axis,...  7.92 us
    all_to_all x1, waiting for transfers between devices, per_device(): lax.all_to_all(branch, 'tp', split_axis=0, concat_axis=1, tiled=True)  7.42 us
  transfers between devices with their start and end apart: 5, of which 4 were waited for; matrix products, arithmetic and copies ran while one was open for 1% of the time, Pallas kernels for 0%

commit v1 on v0

--- a/solution.py
+++ b/solution.py
@@ -1,9 +1,440 @@
+import functools
+
 import jax
 import jax.numpy as jnp
 from jax import lax
+from jax.experimental import pallas as pl
+from jax.experimental.pallas import tpu as pltpu
 from jax.sharding import PartitionSpec as P
 
 EPSILON = 1e-06
+MESH = pl.DeviceIdType.MESH
+F32 = jnp.float32
+BF16 = jnp.bfloat16
+
+SPAN = 4
+PLANES = 16
+GROUPS = 4
+HOPS = 9
+SEATS = 8
+DEPTH = 4
+UNIT = 32
+BLOCKS = 3 + 2 * (HOPS - 1)
+
+
+def first_block(hop):
+    return 0 if hop == 1 else 3 + 2 * (hop - 2)
+
+
+def kinds_at(hop):
+    found = []
+    for rel in (2, 1, 0):
+        if rel == 2 and hop > 1:
+            continue
+        if any(static_valid(on, hop, rel) for on in range(SPAN)):
+            found.append(rel)
+    return found
+
+
+def static_valid(on, hop, rel):
+    start = (on - hop) % SPAN
+    kind = (start + hop) // SPAN + rel
+    return kind <= 1 or (kind == 2 and start >= 2)
+
+
+def valid(on, hop, rel):
+    start = lax.rem(on + 12 - hop, SPAN)
+    kind = lax.div(start + hop, SPAN) + rel
+    return (kind <= 1) | ((kind == 2) & (start >= 2))
+
+
+def iota(shape, dim):
+    return lax.broadcasted_iota(jnp.int32, shape, dim)
+
+
+def ranks(col, row):
+    size = col.shape[0]
+    out = {}
+    e1c, e2c = col[:, 0:1], col[:, 1:2]
+    e1r, e2r = row[0:1, :], row[1:2, :]
+    gc, gr = e1c >> 5, e1r >> 5
+    o1c, o2c = (e1c >> 3) & 3, (e2c >> 3) & 3
+    o1r, o2r = (e1r >> 3) & 3, (e2r >> 3) & 3
+    mxc, mnc = jnp.maximum(o1c, o2c), jnp.minimum(o1c, o2c)
+    mxr, mnr = jnp.maximum(o1r, o2r), jnp.minimum(o1r, o2r)
+    sub = iota((size, size), 0)
+    lane = iota((size, size), 1)
+    same = gc == gr
+    for name, kc, kr in (("P", 3 - mxc, 3 - mxr), ("M", mnc, mnr)):
+        kc = kc * size + iota((size, 1), 0)
+        kr = kr * size + iota((1, size), 1)
+        out[name + "r"] = jnp.sum((same & (kc < kr)).astype(F32), axis=0, keepdims=True).astype(jnp.int32)
+        out[name + "c"] = jnp.sum((same & (kr < kc)).astype(F32), axis=1, keepdims=True).astype(jnp.int32)
+    out.update(gc=gc, gr=gr, mxc=mxc, mnc=mnc, sub=sub, lane=lane)
+    return out
+
+
+def route_body(col_ref, row_ref, wcol_ref, meta_ref):
+    col, row = col_ref[...], row_ref[...]
+    size = col.shape[0]
+    zed = lax.div(lax.axis_index("sp"), 2)
+    zo, g0 = lax.rem(zed, SPAN), lax.div(zed, SPAN)
+    r = ranks(col, row)
+    e1c, e2c = col[:, 0:1], col[:, 1:2]
+    e1r, e2r = row[0:1, :], row[1:2, :]
+    earlier = r["lane"] < r["sub"]
+    place = []
+    for e in (e1c, e2c):
+        hit = ((e == e1r) | (e == e2r)) & earlier
+        place.append(jnp.sum(hit.astype(F32), axis=1, keepdims=True).astype(jnp.int32))
+    group = r["gc"]
+    ahead = group - g0
+    ahead = jnp.where(ahead < 0, ahead + GROUPS, ahead)
+    far_up = jnp.where(zo >= 2, 1, 0)
+    lanes = iota((size, 128), 1)
+    for plane in range(PLANES):
+        slot_row = jnp.full((1, 128), -1.0, F32)
+        weight_row = jnp.zeros((1, 128), F32)
+        for k, e in enumerate((e1c, e2c)):
+            po = plane % SPAN
+            own_up = jnp.where(po >= zo, 1, 0)
+            up = jnp.where(ahead == 0, own_up, jnp.where(ahead == 1, 1, jnp.where(ahead == 2, far_up, 0)))
+            slot = jnp.where(up == 1, r["Pc"], r["Mc"]).astype(F32)
+            lane = jnp.where((e >> 3) == plane, (e & 7) * 16 + place[k], -1)
+            hit = lane == lanes
+            slot_row = slot_row + jnp.sum(jnp.where(hit, slot + 1.0, 0.0), axis=0, keepdims=True)
+            weight_row = weight_row + jnp.sum(jnp.where(hit, wcol_ref[:, k : k + 1], 0.0), axis=0, keepdims=True)
+        meta_ref[plane] = jnp.concatenate([slot_row, weight_row, jnp.zeros((6, 128), F32)], axis=0)
+
+
+def moe_body(
+    hidden_ref, normed_ref, col_ref, row_ref, meta_ref, wg_hbm, wu_hbm, wd_hbm, out_ref,
+    wg, wu, wd, own, came, back, part, xs, xr, rb, yr,
+    wsem, fsend, frecv, bsend, brecv, xsend, xrecv, ysend, yrecv,
+):
+    sp, tp = lax.axis_index("sp"), lax.axis_index("tp")
+    zed, core = lax.div(sp, 2), lax.rem(sp, 2)
+    zo, g0 = lax.rem(zed, SPAN), lax.div(zed, SPAN)
+    seat = core * 4 + tp
+    off = (zo, SPAN - 1 - zo)
+    last = tuple(jnp.where(o == SPAN - 1, 1, 0) for o in off)
+    following = tuple(lax.rem(o + 1, SPAN) for o in off)
+    ring_to = ({"sp": lax.rem(zed + 1, PLANES) * 2 + core}, {"sp": lax.rem(zed + PLANES - 1, PLANES) * 2 + core})
+    ring_from = (ring_to[1], ring_to[0])
+
+    def seat_device(s):
+        return {"sp": zed * 2 + lax.div(s, 4), "tp": lax.rem(s, 4)}
+
+    weights = [
+        pltpu.make_async_copy(wg_hbm.at[0], wg, wsem.at[0]),
+        pltpu.make_async_copy(wu_hbm.at[0], wu, wsem.at[1]),
+        pltpu.make_async_copy(wd_hbm.at[0], wd, wsem.at[2]),
+    ]
+    for w in weights:
+        w.start()
+
+    for d in (0, 1):
+        for i in range(3):
+            back[d, i] = jnp.zeros(back.shape[2:], BF16)
+
+        @pl.when(off[d] == SPAN - 1)
+        def _():
+            for hop in range(1, HOPS + 1):
+                came[d, first_block(hop), 1] = jnp.zeros(came.shape[3:], BF16)
+
+    barrier = pltpu.get_barrier_semaphore()
+    for to in ring_to:
+        pl.semaphore_signal(barrier, inc=1, device_id=to, device_id_type=MESH)
+    for k in range(1, SEATS):
+        pl.semaphore_signal(barrier, inc=1, device_id=seat_device(lax.rem(seat + k, SEATS)), device_id_type=MESH)
+    pl.semaphore_wait(barrier, SEATS + 1)
+
+    r = ranks(col_ref[...], row_ref[...])
+    normed = normed_ref[...]
+    tokens = normed.shape[0]
+    for d, name in ((0, "P"), (1, "M")):
+        slot = r["gr"] * 64 + r[name + "r"]
+        onehot = jnp.where(iota((GROUPS * 64, tokens), 0) == slot, 1.0, 0.0).astype(BF16)
+        rows = jnp.dot(onehot, normed, preferred_element_type=F32).astype(BF16)
+        own[d] = rows.reshape(own.shape[1:])
+
+    def forward(d, src, hop, index, unit):
+        return pltpu.make_async_remote_copy(
+            src_ref=src, dst_ref=came.at[d, index, unit],
+            send_sem=fsend.at[d, index, unit], recv_sem=frecv.at[d, index, unit],
+            device_id=ring_to[d], device_id_type=MESH,
+        )
+
+    def backward(d, src, index, unit):
+        return pltpu.make_async_remote_copy(
+            src_ref=src, dst_ref=back.at[d, index, unit],
+            send_sem=bsend.at[d, index, unit], recv_sem=brecv.at[d, index, unit],
+            device_id=ring_from[d], device_id_type=MESH,
+        )
+
+    def first_hop(act):
+        for rel in kinds_at(1):
+            for unit in (0, 1):
+                for d in (0, 1):
+                    kind = rel + last[d]
+                    group = lax.rem(g0 + kind, GROUPS) if d == 0 else lax.rem(g0 + GROUPS - kind, GROUPS)
+                    fine = valid(following[d], 1, rel)
+                    if unit == 1 and rel == 0:
+                        fine = fine & (following[d] < SPAN - 1)
+
+                    @pl.when(fine)
+                    def _():
+                        act(forward(d, own.at[d, group, unit], 1, rel, unit), d, rel, unit)
+
+    first_hop(lambda copy, *_: copy.start())
+
+    def arrivals(hop, act):
+        for rel in kinds_at(hop):
+            for unit in (0, 1):
+                for d in (0, 1):
+                    fine = valid(off[d], hop, rel)
+                    if unit == 1 and rel == 0:
+                        fine = fine & (off[d] < SPAN - 1)
+
+                    @pl.when(fine)
+                    def _():
+                        act(d, rel, unit)
+
+    def goes_on(d, hop, rel, unit):
+        there = rel - last[d]
+        ok = there >= 0
+        if unit == 1:
+            ok = ok & ((there > 0) | (following[d] < SPAN - 1))
+        return ok, first_block(hop + 1) + jnp.maximum(there, 0)
+
+    def relay(hop):
+        def act(d, rel, unit):
+            index = first_block(hop) + rel
+            forward(d, came.at[d, index, unit], hop, index, unit).wait_recv()
+            if hop < HOPS:
+                ok, there = goes_on(d, hop, rel, unit)
+
+                @pl.when(ok)
+                def _():
+                    forward(d, came.at[d, index, unit], hop + 1, there, unit).start()
+
+        arrivals(hop, act)
+
+    def up_if(flag, a, b):
+        return (jnp.where(flag, a[0], b[0]), jnp.where(flag, first_block(a[1]), first_block(b[1])),
+                jnp.where(flag, zed - a[1], zed + b[1]))
+
+    def fixed(d, hop):
+        return (d, first_block(hop), zed - hop if d == 0 else zed + hop)
+
+    batches = [[fixed(0, h), fixed(1, h), fixed(0, h + 1), fixed(1, h + 1)] for h in (1, 3, 5)]
+    batches.append([
+        None,
+        up_if(zo != 0, (0, 7), (1, 9)),
+        up_if(zo >= 2, (0, 8), (1, 8)),
+        up_if(zo == 3, (0, 9), (1, 7)),
+    ])
+
+    def where_part(d, hop):
+        if hop <= 6:
+            return (hop - 1) // 2, ((hop - 1) % 2) * 2 + d
+        return 3, {(0, 7): 1, (1, 9): 1, (0, 8): 2, (1, 8): 2, (1, 7): 3, (0, 9): 3}[(d, hop)]
+
+    def selectors(b):
+        slots, loads = [], []
+        for k, source in enumerate(batches[b]):
+            whose = zed if source is None else lax.rem(source[2] + PLANES, PLANES)
+            meta = meta_ref[whose]
+            if k:
+                meta = pltpu.roll(meta, 4 * k, 1)
+            slots.append(iota((64, 128), 0).astype(F32) == meta[0:1])
+            loads.append(meta[1:2])
+        return slots, loads
+
+    def spread(b):
+        slots, _ = selectors(b)
+        pick = jnp.concatenate([jnp.where(s, 1.0, 0.0) for s in slots], axis=0)
+        pick = jnp.transpose(pick, (1, 0)).astype(BF16)
+        blocks = []
+        for source in batches[b]:
+            ref = own.at[0, g0] if source is None else came.at[source[0], source[1]]
+            blocks.append(ref[...].reshape(64, ref.shape[-1]))
+        rows = jnp.dot(pick, jnp.concatenate(blocks, axis=0), preferred_element_type=F32)
+        xs[b] = rows.astype(BF16).reshape(xs.shape[1:])
+        pltpu.make_async_copy(xs.at[b, seat], xr.at[b, seat], xrecv.at[b]).start()
+        for k in range(1, SEATS):
+            spread_copy(b, k).start()
+
+    def spread_copy(b, k):
+        to = lax.rem(seat + k, SEATS)
+        return pltpu.make_async_remote_copy(
+            src_ref=xs.at[b, to], dst_ref=xr.at[b, seat], send_sem=xsend.at[b, k], recv_sem=xrecv.at[b],
+            device_id=seat_device(to), device_id_type=MESH,
+        )
+
+    def return_copy(b, k):
+        to = lax.rem(seat + k, SEATS)
+        return pltpu.make_async_remote_copy(
+            src_ref=rb.at[b, to], dst_ref=yr.at[b, seat], send_sem=ysend.at[b, k], recv_sem=yrecv.at[b],
+            device_id=seat_device(to), device_id_type=MESH,
+        )
+
+    def expert(b):
+        pltpu.make_async_copy(xs.at[b], xr.at[b], xrecv.at[b]).wait()
+        rows = xr[b].reshape(SEATS * 16, xr.shape[-1])
+        gate = jnp.dot(rows, wg[...], preferred_element_type=F32)
+        up = jnp.dot(rows, wu[...], preferred_element_type=F32)
+        active = (jax.nn.silu(gate) * up).astype(BF16)
+        result = jnp.dot(active, wd[...], preferred_element_type=F32).astype(BF16)
+        rb[b] = result.reshape(rb.shape[1:])
+        pltpu.make_async_copy(rb.at[b, seat], yr.at[b, seat], yrecv.at[b]).start()
+        for k in range(1, SEATS):
+            return_copy(b, k).start()
+
+    def combine(b):
+        slots, loads = selectors(b)
+        pltpu.make_async_copy(rb.at[b], yr.at[b], yrecv.at[b]).wait()
+        rows = yr[b].reshape(SEATS * 16, yr.shape[-1])
+        scale = jnp.concatenate([jnp.where(s, w, 0.0) for s, w in zip(slots, loads)], axis=0)
+        high = scale.astype(BF16)
+        low = (scale - high.astype(F32)).astype(BF16)
+        total = jnp.dot(high, rows, preferred_element_type=F32) + jnp.dot(low, rows, preferred_element_type=F32)
+        part[b] = total.astype(BF16).reshape(part.shape[1:])
+
+    relay(1)
+    relay(2)
+    spread(0)
+    relay(3)
+    relay(4)
+    spread(1)
+    for w in weights:
+        w.wait()
+    expert(0)
+    relay(5)
+    relay(6)
+    spread(2)
+    expert(1)
+    combine(0)
+    relay(7)
+    relay(8)
+    relay(9)
+    spread(3)
+    expert(2)
+    combine(1)
+    expert(3)
+    combine(2)
+    combine(3)
+
+    def hand_back(hop):
+        for rel in reversed(kinds_at(hop)):
+            for unit in (0, 1):
+                for d in (0, 1):
+                    fine = valid(off[d], hop, rel)
+                    if unit == 1 and rel == 0:
+                        fine = fine & (off[d] < SPAN - 1)
+                    index = first_block(hop) + rel
+                    b, k = where_part(d, hop) if rel == 0 else (0, 0)
+
+                    @pl.when(fine)
+                    def _():
+                        if rel == 0:
+                            if hop < HOPS:
+                                later = first_block(hop + 1)
+
+                                @pl.when(off[d] < SPAN - 1 - unit)
+                                def _():
+                                    backward(d, back.at[d, later, unit], later, unit).wait_recv()
+                                    part[b, k, unit] = (
+                                        part[b, k, unit].astype(F32) + back[d, later, unit].astype(F32)
+                                    ).astype(BF16)
+
+                            backward(d, part.at[b, k, unit], index, unit).start()
+                        else:
+                            later = first_block(hop + 1) + rel - last[d]
+                            backward(d, back.at[d, later, unit], later, unit).wait_recv()
+                            backward(d, back.at[d, later, unit], index, unit).start()
+
+    for hop in range(HOPS, 0, -1):
+        hand_back(hop)
+
+    first_hop(lambda copy, d, rel, unit: backward(d, back.at[d, rel, unit], rel, unit).wait_recv())
+    group, up_rank, down_rank = r["gc"], r["Pc"], r["Mc"]
+    lanes = iota((tokens, 64), 1)
+    far = jnp.where(zo >= 2, 0, 1)
+    far_rank = jnp.where(zo >= 2, up_rank, down_rank)
+    plan = [
+        ((group == g0) & (r["mxc"] > zo), up_rank, back.at[0, 0]),
+        ((group == g0) & (r["mnc"] < zo), down_rank, back.at[1, 0]),
+        (group == lax.rem(g0 + 1, GROUPS), up_rank, back.at[0, 1 - last[0]]),
+        (group == lax.rem(g0 + GROUPS - 1, GROUPS), down_rank, back.at[1, 1 - last[1]]),
+        (group == lax.rem(g0 + 2, GROUPS), far_rank, back.at[far, 2 - jnp.where(zo >= 2, last[0], last[1])]),
+        (group == g0, up_rank, part.at[3, 0]),
+    ]
+    pick = [jnp.where((jnp.where(mask, rank, -1) == lanes), 1.0, 0.0) for mask, rank, _ in plan]
+    pick = jnp.concatenate(pick, axis=1).astype(BF16)
+    blocks = jnp.concatenate([ref[...].reshape(64, ref.shape[-1]) for _, _, ref in plan], axis=0)
+    total = jnp.dot(pick, blocks, preferred_element_type=F32)
+    out_ref[...] = (hidden_ref[...].astype(F32) + total).astype(BF16)
+
+    first_hop(lambda copy, *_: copy.wait_send())
+    for hop in range(1, HOPS + 1):
+        def done(d, rel, unit):
+            index = first_block(hop) + rel
+            if hop < HOPS:
+                ok, there = goes_on(d, hop, rel, unit)
+
+                @pl.when(ok)
+                def _():
+                    forward(d, came.at[d, index, unit], hop + 1, there, unit).wait_send()
+
+            backward(d, back.at[d, index, unit], index, unit).wait_send()
+
+        arrivals(hop, done)
+    for b in range(len(batches)):
+        for k in range(1, SEATS):
+            spread_copy(b, k).wait_send()
+            return_copy(b, k).wait_send()
+
+
+def route(ids, loads):
+    size = ids.shape[0]
+    return pl.pallas_call(
+        route_body,
+        out_shape=jax.ShapeDtypeStruct((PLANES, 8, 128), F32),
+        in_specs=[pl.BlockSpec(memory_space=pltpu.VMEM)] * 3,
+        out_specs=pl.BlockSpec(memory_space=pltpu.VMEM),
+    )(ids, ids.T, loads)
+
+
+def experts_kernel(hidden, normed, ids, meta, w_gate, w_up, w_down):
+    rows, width = normed.shape
+    inner = w_gate.shape[2]
+    vmem = pl.BlockSpec(memory_space=pltpu.VMEM)
+    far = pl.BlockSpec(memory_space=pl.ANY)
+    seats = pltpu.VMEM((4, SEATS, 16, width), BF16)
+    dma = pltpu.SemaphoreType.DMA
+    return pl.pallas_call(
+        moe_body,
+        out_shape=jax.ShapeDtypeStruct((rows, width), BF16),
+        in_specs=[vmem] * 5 + [far] * 3,
+        out_specs=vmem,
+        scratch_shapes=[
+            pltpu.VMEM((width, inner), BF16),
+            pltpu.VMEM((width, inner), BF16),
+            pltpu.VMEM((inner, width), BF16),
+            pltpu.VMEM((2, GROUPS, 2, UNIT, width), BF16),
+            pltpu.VMEM((2, BLOCKS, 2, UNIT, width), BF16),
+            pltpu.VMEM((2, BLOCKS, 2, UNIT, width), BF16),
+            pltpu.VMEM((4, 4, 2, UNIT, width), BF16),
+            seats, seats, seats, seats,
+            dma((3,)),
+            dma((2, BLOCKS, 2)), dma((2, BLOCKS, 2)), dma((2, BLOCKS, 2)), dma((2, BLOCKS, 2)),
+            dma((4, SEATS)), dma((4,)), dma((4, SEATS)), dma((4,)),
+        ],
+        compiler_params=pltpu.CompilerParams(
+            collective_id=1, has_side_effects=True, vmem_limit_bytes=60 << 20
+        ),
+    )(hidden, normed, ids, ids.T, meta, w_gate, w_up, w_down)
 
 
 def passed_along(block, axis, distance):
@@ -77,31 +508,13 @@
     normed = (
         widened * lax.rsqrt(jnp.mean(widened * widened, axis=1, keepdims=True) + EPSILON) * moe_gain
     ).astype(jnp.bfloat16)
-    width = normed.shape[1]
-    experts = lax.axis_size("sp") * lax.axis_size("tp")
-    capacity = 2 * row_count // min(row_count, experts // 2)
-    flat_ids = expert_ids.reshape(-1)
-    onehot = (flat_ids[:, None] == jnp.arange(experts, dtype=jnp.int32)[None, :]).astype(jnp.int32)
-    slot_rank = jnp.sum((jnp.cumsum(onehot, axis=0) - 1) * onehot, axis=1)
-    position = flat_ids * capacity + slot_rank
-    outgoing = (
-        jnp.zeros((experts * capacity, width), jnp.bfloat16)
-        .at[position]
-        .set(jnp.repeat(normed, 2, axis=0))
+    meta = route(expert_ids, expert_weights)
+    cores = jnp.repeat(meta, 2, axis=0)
+    shared = lax.all_to_all(cores, "sp", split_axis=0, concat_axis=0, tiled=True)
+    mine = lax.dynamic_index_in_dim(
+        shared.reshape(PLANES, 2, *meta.shape[1:]), lax.axis_index("sp") % 2, axis=1, keepdims=False
     )
-    outgoing = outgoing.reshape(experts, capacity, width)
-    arriving = lax.all_to_all(outgoing, ("sp", "tp"), split_axis=0, concat_axis=0, tiled=True)
-    flattened = arriving.reshape(-1, width)
-    gate_part = jnp.dot(flattened, w_gate[0], preferred_element_type=jnp.float32)
-    up_part = jnp.dot(flattened, w_up[0], preferred_element_type=jnp.float32)
-    active = (jax.nn.silu(gate_part) * up_part).astype(jnp.bfloat16)
-    result = jnp.dot(active, w_down[0], preferred_element_type=jnp.float32).astype(jnp.bfloat16)
-    produced = result.reshape(arriving.shape)
-    returned = lax.all_to_all(produced, ("sp", "tp"), split_axis=0, concat_axis=0, tiled=True)
-    returned = returned.reshape(experts * capacity, width)
-    picked = returned[position].reshape(row_count, 2, width)
-    combined = jnp.sum(picked.astype(jnp.float32) * expert_weights[:, :, None], axis=1)
-    return (widened + combined).astype(jnp.bfloat16)
+    return experts_kernel(hidden, normed, expert_ids, mine, w_gate, w_up, w_down)
 
 
 def solution(mesh):

time: 330 us -> 254 us (0.77)
  Pallas kernels: 0 us -> 170 us
  blocking collectives: 125 us -> 17.4 us
  waiting for transfers between devices: 113 us -> 15.1 us
  local copies, waits for them, and re-layouts: 36 us -> 5.67 us
  matrix products: 13.8 us -> 3.03 us
  starting transfers between devices: 25.7 us -> 30.4 us
  other arithmetic: 14.3 us -> 10.1 us
    pallas_call x0 -> x2, Pallas kernels: none -> 170 us  [the longest x1 167 us: experts_kernel(): pl.pallas_call(moe_body, out_shape=jax.ShapeDtypeStruct((rows, width), BF...]
    all_to_all x1 -> x2, blocking collectives: 125 us -> 17.4 us  [copy_for_each(): lax.all_to_all(jnp.broadcast_to(shard[None], (size, *shard.shape)), axis,...]
    all_to_all x3 -> x1, waiting for transfers between devices: 105 us -> 12.3 us  [per_device(): lax.all_to_all(cores, 'sp', split_axis=0, concat_axis=0, tiled=True)]
    reshape x5 -> x0, local copies, waits for them, and re-layouts: 18.4 us -> none  [the longest x1 4.12 us: per_device(): outgoing = outgoing.reshape(experts, capacity, width)]
    dot_general x2 -> x0, matrix products: 10.7 us -> none  [the longest x1 6.22 us: per_device(): jnp.dot(active, w_down[0], preferred_element_type=jnp.float32)]
    gather x1 -> x0, local copies, waits for them, and re-layouts: 5.2 us -> none  [per_device(): picked = returned[position].reshape(row_count, 2, width)]
    reduce_sum x2 -> x0, other arithmetic: 4.99 us -> none  [the longest x1 4.81 us: per_device(): jnp.sum(picked.astype(jnp.float32) * expert_weights[:, :, None], axis=1)]
    all_to_all x3 -> x1, starting transfers between devices: 20.3 us -> 25.1 us  [per_device(): lax.all_to_all(cores, 'sp', split_axis=0, concat_axis=0, tiled=True)]
  transfers between devices with their start and end apart: 5 -> 3, of which waited for: 4 -> 2; matrix products, arithmetic and copies ran while one was open for 1% -> 3% of each run, Pallas kernels for 0% -> 1%
where the time goes in v1:
time: 254 us; the launch traced here: 252 us
  Pallas kernels  170 us (67%)
  starting transfers between devices  30.4 us (12%)
  blocking collectives  17.4 us (7%)
  waiting for transfers between devices  15.1 us (6%)
  other arithmetic  10.1 us (4%)
  local copies, waits for them, and re-layouts  5.67 us (2%)
  matrix products  3.03 us (1%)
    pallas_call x1, Pallas kernels, experts_kernel(): pl.pallas_call(moe_body, out_shape=jax.ShapeDtypeStruct((rows, width), BF...  167 us
    all_to_all x1, starting transfers between devices, per_device(): lax.all_to_all(cores, 'sp', split_axis=0, concat_axis=0, tiled=True)  25.1 us
    all_to_all x2, blocking collectives, copy_for_each(): lax.all_to_all(jnp.broadcast_to(shard[None], (size, *shard.shape)), axis,...  17.4 us
    all_to_all x1, waiting for transfers between devices, per_device(): lax.all_to_all(cores, 'sp', split_axis=0, concat_axis=0, tiled=True)  12.3 us
  transfers between devices with their start and end apart: 3, of which 2 were waited for; matrix products, arithmetic and copies ran while one was open for 3% of the time, Pallas kernels for 1%

profile of v1, /device:TPU:40, one launch (start us, length us, event | category | flops | bytes accessed | tf_op | source)
XLA Modules:
  0.0 251.6 jit_solution(10976238424617447151)
XLA Ops:
  0.0 1.2 multiply_convert_fusion.1
  1.3 1.8 collective-permute-start
  3.1 1.0 slice_convert_fusion.30
  4.1 1.0 slice_convert_fusion.29
  5.1 3.2 %fusion.33 = (f32[512]{0:T(512)S(1)}, f32[512]{0:T(512)S(1)}, f32[512,256]{1,0:T(8,128)S(1)}) fusion(f32[256]{0:T(256)S(1)} %bitcast.75, bf16[512,256]{1,0:T(8,128)(2,1)S(1)} %multiply_convert_fusion.1, f32[256]{0:T(256)S(1)} %bitcast.76, bf16[30,256]{1,0:T(8,128)(2,1)S(1)} %collective-permute-done, f32[256]{0:T(256)S(1)} %bitcast.47, f32[256]{0:T(256)S(1)} %bitcast.48, ...), kind=kLoop, calls=%fused_computation.114 | loop fusion | flops 24378368 | bytes 838656 | tf_op jit(solution)/shard_map/reduce_sum | solution.py:495
  8.4 9.7 %all_to_all.36 = f32[4,1,1024]{2,1,0:T(1,128)S(1)} all-to-all(f32[4,1,1024]{2,1,0:T(1,128)S(1)} %broadcast_in_dim.6), channel_id=1, replica_groups=mesh['grp'=2,'sp'=32,'tp'=4] {'tp'}, dimensions={0} | all-to-all | bytes 32768 | tf_op jit(solution)/shard_map/all_to_all | solution.py:448
  18.2 1.0 multiply_reduce_fusion
  19.2 0.0 copy-start.3
  19.2 7.7 %all_to_all.37 = f32[4,1,512]{2,1,0:T(1,128)S(1)} all-to-all(f32[4,1,512]{2,1,0:T(1,128)S(1)} %broadcast_in_dim.7), channel_id=1, replica_groups=mesh['grp'=2,'sp'=32,'tp'=4] {'tp'}, dimensions={0} | all-to-all | bytes 16384 | tf_op jit(solution)/shard_map/all_to_all | solution.py:448
  27.0 1.5 multiply_convert_fusion
  28.5 3.5 %all-to-all-start.2 = ((bf16[4,128,256]{2,1,0:T(8,128)(2,1)}), bf16[4,128,256]{2,1,0:T(8,128)(2,1)S(1)}, u32[]{:S(2)}, u32[]{:S(2)}) async-start(bf16[4,128,256]{2,1,0:T(8,128)(2,1)} %bitcast.31), calls=%async_computation.2 | async-start | bytes 524288 | tf_op jit(solution)/shard_map/all_to_all | solution.py:504
  32.0 0.7 copy.35.col_ref
  32.7 0.7 copy.34.wcol_ref
  33.5 3.2 %shard_map.145 = f32[16,8,128]{2,1,0:T(8,128)} custom-call(s32[128,2]{1,0:T(8,128)} %copy.35.col_ref, s32[2,128]{1,0:T(2,128)} %bitcast.44, f32[128,2]{1,0:T(8,128)} %copy.34.wcol_ref), custom_call_target="tpu_custom_call" | custom-call | tf_op jit(solution)/shard_map/pallas_call | solution.py:401
  36.6 2.8 %all-to-all-done.2 = bf16[4,128,256]{2,1,0:T(8,128)(2,1)S(1)} async-done(((bf16[4,128,256]{2,1,0:T(8,128)(2,1)}), bf16[4,128,256]{2,1,0:T(8,128)(2,1)S(1)}, u32[]{:S(2)}, u32[]{:S(2)}) %all-to-all-start.2) | async-done | bytes 262176 | tf_op jit(solution)/shard_map/all_to_all | solution.py:504
  39.4 1.5 broadcast_in_dim.8
  40.9 25.1 %all-to-all-start.3 = ((f32[32,8,128]{2,1,0:T(8,128)}), f32[32,8,128]{2,1,0:T(8,128)S(1)}, u32[]{:S(2)}, u32[]{:S(2)}) async-start(f32[32,8,128]{2,1,0:T(8,128)} %bitcast.35), calls=%async_computation.3 | async-start | bytes 262144 | tf_op jit(solution)/shard_map/all_to_all | solution.py:513
  66.0 0.2 copy.32
  66.2 3.0 %fusion.1 = (f32[128]{0:T(128)S(1)}, bf16[128,2048]{1,0:T(8,128)(2,1)S(1)}) fusion(bf16[128,1024]{0,1:T(8,128)(2,1)S(1)} %bitcast.41, bf16[1024,2048]{1,0:T(8,128)(2,1)} %param.22, bf16[128,2048]{1,0:T(8,128)(2,1)S(1)} %copy-done.1), kind=kOutput, calls=%fused_computation.33 | convolution fusion | flops 538443648 | bytes 5505536 | tf_op jit(solution)/shard_map/dot_general | solution.py:505
  69.2 1.0 fusion.3.normed_ref
  70.2 12.3 %all-to-all-done.3 = f32[32,8,128]{2,1,0:T(8,128)S(1)} async-done(((f32[32,8,128]{2,1,0:T(8,128)}), f32[32,8,128]{2,1,0:T(8,128)S(1)}, u32[]{:S(2)}, u32[]{:S(2)}) %all-to-all-start.3) | async-done | bytes 131104 | tf_op jit(solution)/shard_map/all_to_all | solution.py:513
  82.5 0.6 dynamic-slice_bitcast_fusion.meta_ref
  83.1 166.6 %shard_map.146 = bf16[128,2048]{1,0:T(8,128)(2,1)} custom-call(bf16[128,2048]{1,0:T(8,128)(2,1)} %copy-done, bf16[128,2048]{1,0:T(8,128)(2,1)} %fusion.3.normed_ref, s32[128,2]{1,0:T(8,128)} %copy.35.col_ref, s32[2,128]{1,0:T(2,128)} %bitcast.45, f32[16,8,128]{2,1,0:T(8,128)} %dynamic-slice_bitcast_fusion.meta_ref, bf16[1,2048,512]{2,1,0:T(8,128)(2,1)} %wg_hbm.1, ...), custom_call_target="tpu_custom_call" | custom-call | tf_op jit(solution)/shard_map/pallas_call | solution.py:416
  249.7 1.9 copy.41
  (19 shorter events, 0.1 us)
Async XLA Ops:
  0.0 32.0 %copy-start.2 = (s32[128,2]{0,1:T(2,128)S(1)}, s32[128,2]{0,1:T(2,128)}, u32[]{:S(2)}) copy-start(s32[128,2]{0,1:T(2,128)} %param.25) | copy-start | bytes 3076
  0.0 32.7 %copy-start.4 = (f32[128,2]{0,1:T(2,128)S(1)}, f32[128,2]{0,1:T(2,128)}, u32[]{:S(2)}) copy-start(f32[128,2]{0,1:T(2,128)} %param.26) | copy-start | bytes 3076
  0.0 66.2 %copy-start.1 = (bf16[128,2048]{1,0:T(8,128)(2,1)S(1)}, bf16[128,2048]{1,0:T(8,128)(2,1)}, u32[]{:S(2)}) copy-start(bf16[128,2048]{1,0:T(8,128)(2,1)} %param.23) | copy-start | bytes 1572868
  1.3 3.8 %collective-permute-start = (bf16[30,256]{1,0:T(8,128)(2,1)S(1)}, bf16[30,256]{1,0:T(8,128)(2,1)S(1)}, u32[]{:S(2)}, u32[]{:S(2)}) collective-permute-start(bf16[30,256]{1,0:T(8,128)(2,1)S(1)} %slice.256), channel_id=1, source_target_pairs={{0,4},{4,8},{8,12},{12,16},{16,20},{20,24},{24,28},{28,32},{32,36}... | collective-permute-start | bytes 46088 | tf_op jit(solution)/shard_map/ppermute | solution.py:443
  19.2 50.0 %copy-start.3 = (f32[2048]{0:T(1024)S(1)}, f32[2048]{0:T(1024)}, u32[]{:S(2)}) copy-start(f32[2048]{0:T(1024)} %param.24) | copy-start | bytes 24580
  28.5 10.9 %all-to-all-start.2 = ((bf16[4,128,256]{2,1,0:T(8,128)(2,1)}), bf16[4,128,256]{2,1,0:T(8,128)(2,1)S(1)}, u32[]{:S(2)}, u32[]{:S(2)}) async-start(bf16[4,128,256]{2,1,0:T(8,128)(2,1)} %bitcast.31), calls=%async_computation.2 | async-start | bytes 524288 | tf_op jit(solution)/shard_map/all_to_all | solution.py:504
  40.9 41.6 %all-to-all-start.3 = ((f32[32,8,128]{2,1,0:T(8,128)}), f32[32,8,128]{2,1,0:T(8,128)S(1)}, u32[]{:S(2)}, u32[]{:S(2)}) async-start(f32[32,8,128]{2,1,0:T(8,128)} %bitcast.35), calls=%async_computation.3 | async-start | bytes 262144 | tf_op jit(solution)/shard_map/all_to_all | solution.py:513
  69.2 13.9 %copy-start = (bf16[128,2048]{1,0:T(8,128)(2,1)}, bf16[128,2048]{1,0:T(8,128)(2,1)S(1)}, u32[]{:S(2)}) copy-start(bf16[128,2048]{1,0:T(8,128)(2,1)S(1)} %get-tuple-element.44.hidden_ref) | copy-start | bytes 1572868

commit v2 on v1

--- a/solution.py
+++ b/solution.py
@@ -1,5 +1,3 @@
-import functools
-
 import jax
 import jax.numpy as jnp
 from jax import lax
@@ -17,7 +15,6 @@
 GROUPS = 4
 HOPS = 9
 SEATS = 8
-DEPTH = 4
 UNIT = 32
 BLOCKS = 3 + 2 * (HOPS - 1)
 
@@ -74,10 +71,9 @@
     return out
 
 
-def route_body(col_ref, row_ref, wcol_ref, meta_ref):
+def route_body(col_ref, row_ref, wcol_ref, meta_ref, zed):
     col, row = col_ref[...], row_ref[...]
     size = col.shape[0]
-    zed = lax.div(lax.axis_index("sp"), 2)
     zo, g0 = lax.rem(zed, SPAN), lax.div(zed, SPAN)
     r = ranks(col, row)
     e1c, e2c = col[:, 0:1], col[:, 1:2]
@@ -394,16 +390,6 @@
         for k in range(1, SEATS):
             spread_copy(b, k).wait_send()
             return_copy(b, k).wait_send()
-
-
-def route(ids, loads):
-    size = ids.shape[0]
-    return pl.pallas_call(
-        route_body,
-        out_shape=jax.ShapeDtypeStruct((PLANES, 8, 128), F32),
-        in_specs=[pl.BlockSpec(memory_space=pltpu.VMEM)] * 3,
-        out_specs=pl.BlockSpec(memory_space=pltpu.VMEM),
-    )(ids, ids.T, loads)
 
 
 def experts_kernel(hidden, normed, ids, meta, w_gate, w_up, w_down):
@@ -437,29 +423,229 @@
     )(hidden, normed, ids, ids.T, meta, w_gate, w_up, w_down)
 
 
-def passed_along(block, axis, distance):
-    devices = range(lax.axis_size(axis))
-    route = [(i - distance, i) for i in devices if i - distance in devices]
-    return lax.ppermute(block, axis, route)
-
-
-def copy_for_each(shard, axis):
-    size = lax.axis_size(axis)
-    return lax.all_to_all(
-        jnp.broadcast_to(shard[None], (size, *shard.shape)), axis, 0, 0, tiled=True
-    )
-
-
-def of_everyone(shard, axis):
-    return copy_for_each(shard, axis).sum(axis=0)
-
-
-def together(arrays, axis):
-    ends = [0]
-    for a in arrays:
-        ends.append(ends[-1] + a.size)
-    subtotal = of_everyone(jnp.concatenate([a.ravel() for a in arrays]), axis)
-    return tuple((subtotal[b:e].reshape(a.shape) for a, b, e in zip(arrays, ends, ends[1:])))
+def front_body(
+    value_ref, gate_ref, taps_ref, vec_ref, gain_ref, col_ref, row_ref, load_ref, weight_hbm, residual_hbm,
+    hidden_ref, normed_ref, meta_ref,
+    weight, residual, gated, grown, packs, conv, tables,
+    lsem, gsend, grecv, hsend, hrecv, psend, precv, tsend, trecv,
+):
+    sp, tp = lax.axis_index("sp"), lax.axis_index("tp")
+    steps, teams = lax.axis_size("sp"), lax.axis_size("tp")
+    zed, core = lax.div(sp, 2), lax.rem(sp, 2)
+    rows = hidden_ref.shape[0]
+    pieces = rows // UNIT
+    channels = value_ref.shape[1]
+
+    def team(k):
+        return lax.rem(tp + k, teams)
+
+    def column(k):
+        return lax.rem(zed + k, PLANES) * 2 + core
+
+    barrier = pltpu.get_barrier_semaphore()
+    for k in range(1, teams):
+        pl.semaphore_signal(barrier, inc=1, device_id={"tp": team(k)}, device_id_type=MESH)
+
+    @pl.when((sp > 0) & (tp == 0))
+    def _():
+        for k in range(teams):
+            pl.semaphore_signal(barrier, inc=1, device_id={"sp": sp - 1, "tp": k}, device_id_type=MESH)
+
+    for k in range(1, PLANES):
+        pl.semaphore_signal(barrier, inc=1, device_id={"sp": column(k)}, device_id_type=MESH)
+
+    fetch_weight = pltpu.make_async_copy(weight_hbm, weight, lsem.at[0])
+    fetch_residual = pltpu.make_async_copy(residual_hbm, residual, lsem.at[1])
+    fetch_weight.start()
+    fetch_residual.start()
+
+    passed = (value_ref[...].astype(F32) * jax.nn.sigmoid(gate_ref[...].astype(F32))).astype(BF16)
+    gated[...] = passed.reshape(gated.shape)
+    packs[tp, 0 : taps_ref.shape[0]] = taps_ref[...].astype(F32)
+    packs[tp, 32:40] = vec_ref[...]
+
+    @pl.when((sp == 0) & (tp == 0))
+    def _():
+        grown[:, 0] = jnp.zeros((teams, UNIT, channels), BF16)
+
+    route_body(col_ref, row_ref, load_ref, tables, zed)
+    pl.semaphore_wait(barrier, teams + PLANES - 2 + jnp.where(sp < steps - 1, 1, 0))
+
+    def whole(to, k):
+        return pltpu.make_async_remote_copy(
+            src_ref=gated.at[pl.ds(jnp.maximum(to * pieces - 1, 0), pieces + 1)], dst_ref=grown.at[tp],
+            send_sem=gsend.at[k], recv_sem=grecv.at[tp], device_id={"tp": to}, device_id_type=MESH,
+        )
+
+    def short(to, k):
+        return pltpu.make_async_remote_copy(
+            src_ref=gated.at[pl.ds(0, pieces)], dst_ref=grown.at[tp, pl.ds(1, pieces)],
+            send_sem=gsend.at[k], recv_sem=grecv.at[tp], device_id={"tp": to}, device_id_type=MESH,
+        )
+
+    def got(source, first):
+        size = pieces if first else pieces + 1
+        return pltpu.make_async_remote_copy(
+            src_ref=gated.at[pl.ds(0, size)], dst_ref=grown.at[source, pl.ds(1 if first else 0, size)],
+            send_sem=gsend.at[0], recv_sem=grecv.at[source], device_id={"tp": source}, device_id_type=MESH,
+        )
+
+    def pack_copy(k):
+        return pltpu.make_async_remote_copy(
+            src_ref=packs.at[tp], dst_ref=packs.at[tp], send_sem=psend.at[k], recv_sem=precv.at[tp],
+            device_id={"tp": team(k)}, device_id_type=MESH,
+        )
+
+    def halo(source):
+        return pltpu.make_async_remote_copy(
+            src_ref=gated.at[gated.shape[0] - 1], dst_ref=grown.at[source, 0],
+            send_sem=hsend.at[0], recv_sem=hrecv.at[source],
+            device_id={"sp": lax.rem(sp + 1, steps), "tp": 0}, device_id_type=MESH,
+        )
+
+    def table_copy(k):
+        return pltpu.make_async_remote_copy(
+            src_ref=tables.at[column(k)  // 2], dst_ref=meta_land(k), send_sem=tsend.at[k], recv_sem=trecv.at[k],
+            device_id={"sp": column(k)}, device_id_type=MESH,
+        )
+
+    def meta_land(k):
+        return tables.at[PLANES + k]
+
+    for k in (2, 1, 3):
+        pack_copy(k).start()
+        for test, copy in ((team(k) == 0, short), (team(k) > 0, whole)):
+
+            @pl.when(test)
+            def _():
+                copy(team(k), k).start()
+
+    @pl.when(sp < steps - 1)
+    def _():
+        halo(tp).start()
+
+    for k in range(1, PLANES):
+        table_copy(k).start()
+
+    for test, size in ((tp == 0, 0), (tp > 0, 1)):
+
+        @pl.when(test)
+        def _():
+            low = jnp.maximum(tp * pieces - 1, 0) if size else 0
+            grown[tp, 1 - size : pieces + 1] = gated[pl.ds(low, pieces + size)]
+
+    def wait_part(k):
+        source = team(k)
+        if k:
+            for test, first in ((tp == 0, True), (tp > 0, False)):
+
+                @pl.when(test)
+                def _():
+                    got(source, first).wait_recv()
+
+            pltpu.make_async_remote_copy(
+                src_ref=packs.at[tp], dst_ref=packs.at[source], send_sem=psend.at[k], recv_sem=precv.at[source],
+                device_id={"tp": source}, device_id_type=MESH,
+            ).wait_recv()
+
+        @pl.when((tp == 0) & (sp > 0))
+        def _():
+            halo(source).wait_recv()
+
+    reach = taps_ref.shape[0] - 1
+    shift0 = UNIT - reach
+    for k in (0, 1, 3, 2):
+        wait_part(k)
+        source = team(k)
+        for half in range(channels // 128):
+            lanes = pl.ds(half * 128, 128)
+            x = grown[source, :, :, lanes].reshape((pieces + 1) * UNIT, 128).astype(F32)
+            total = jnp.broadcast_to(packs[source, 32:33, lanes], (rows, 128))
+            for r in range(8):
+                span = rows if r == 0 else rows + 8
+                acc = None
+                for q in range(0, (UNIT - r) // 8 + 1):
+                    tap = 8 * q + r - shift0
+                    if not 0 <= tap <= reach:
+                        continue
+                    term = x[8 * q : 8 * q + span] * packs[source, tap : tap + 1, lanes]
+                    acc = term if acc is None else acc + term
+                total = total + (acc if r == 0 else acc[r : r + rows])
+            conv[source, :, lanes] = total
+
+    full = channels * teams
+    parts = [conv[s] for s in range(teams)]
+    average = sum(jnp.sum(p, axis=1, keepdims=True) for p in parts) / full
+    spread = sum(jnp.sum(p * p, axis=1, keepdims=True) for p in parts) / full - average * average
+    scale = lax.rsqrt(spread + EPSILON)
+    energy = jnp.zeros((rows, 1), F32)
+    for s in range(teams):
+        v = jax.nn.silu((conv[s] - average) * scale * packs[s, 33:34] + packs[s, 34:35])
+        conv[s] = v
+        energy = energy + jnp.sum(v * v, axis=1, keepdims=True)
+    scale = lax.rsqrt(energy / full + EPSILON)
+    branch = jnp.concatenate([(conv[s] * scale * packs[s, 35:36]).astype(BF16) for s in range(teams)], axis=1)
+    fetch_weight.wait()
+    fetch_residual.wait()
+    projected = jnp.dot(branch, weight[...], preferred_element_type=F32)
+    hidden = (residual[...].astype(F32) + projected).astype(BF16)
+    hidden_ref[...] = hidden
+    wide = hidden.astype(F32)
+    scale = lax.rsqrt(jnp.mean(wide * wide, axis=1, keepdims=True) + EPSILON)
+    normed_ref[...] = (wide * scale * gain_ref[...]).astype(BF16)
+
+    meta_ref[zed] = tables[zed]
+    for k in range(1, PLANES):
+        table_copy(k).wait_recv()
+        meta_ref[lax.rem(zed + PLANES - k, PLANES)] = tables[PLANES + k]
+
+    for k in range(1, teams):
+        pack_copy(k).wait_send()
+        for test, copy in ((team(k) == 0, short), (team(k) > 0, whole)):
+
+            @pl.when(test)
+            def _():
+                copy(team(k), k).wait_send()
+
+    @pl.when(sp < steps - 1)
+    def _():
+        halo(tp).wait_send()
+
+    for k in range(1, PLANES):
+        table_copy(k).wait_send()
+
+
+def front_kernel(value, gate, taps, vectors, moe_gain, ids, loads, out_weight, residual):
+    rows, width = residual.shape
+    tok_rows, channels = value.shape
+    teams = lax.axis_size("tp")
+    vmem = pl.BlockSpec(memory_space=pltpu.VMEM)
+    far = pl.BlockSpec(memory_space=pl.ANY)
+    dma = pltpu.SemaphoreType.DMA
+    return pl.pallas_call(
+        front_body,
+        out_shape=(
+            jax.ShapeDtypeStruct((rows, width), BF16),
+            jax.ShapeDtypeStruct((rows, width), BF16),
+            jax.ShapeDtypeStruct((PLANES, 8, 128), F32),
+        ),
+        in_specs=[vmem] * 8 + [far] * 2,
+        out_specs=[vmem] * 3,
+        scratch_shapes=[
+            pltpu.VMEM(out_weight.shape, BF16),
+            pltpu.VMEM((rows, width), BF16),
+            pltpu.VMEM((tok_rows // UNIT, UNIT, channels), BF16),
+            pltpu.VMEM((teams, rows // UNIT + 1, UNIT, channels), BF16),
+            pltpu.VMEM((teams, 40, channels), F32),
+            pltpu.VMEM((teams, rows, channels), F32),
+            pltpu.VMEM((2 * PLANES, 8, 128), F32),
+            dma((2,)), dma((teams,)), dma((teams,)), dma((1,)), dma((teams,)), dma((teams,)), dma((teams,)),
+            dma((PLANES,)), dma((PLANES,)),
+        ],
+        compiler_params=pltpu.CompilerParams(
+            collective_id=2, has_side_effects=True, vmem_limit_bytes=40 << 20
+        ),
+    )(value, gate, taps, vectors, moe_gain, ids, ids.T, loads, out_weight, residual)
 
 
 def per_device(
@@ -479,42 +665,12 @@
     w_up,
     w_down,
 ):
-    tok_rows, channels = conv_value.shape
-    reach_rows = kernel.shape[0] - 1
-    full_channels = channels * lax.axis_size("tp")
-    gated = (conv_value.astype(jnp.float32) * jax.nn.sigmoid(conv_gate.astype(jnp.float32))).astype(
-        jnp.bfloat16
+    nothing = jnp.zeros((4, conv_bias.shape[0]), jnp.float32)
+    vectors = jnp.concatenate([jnp.stack([conv_bias, ln_gain, ln_bias, out_gain]), nothing], axis=0)
+    hidden, normed, meta = front_kernel(
+        conv_value, conv_gate, kernel, vectors, moe_gain[None], expert_ids, expert_weights, out_weight, residual
     )
-    before = passed_along(gated[tok_rows - reach_rows :], "sp", 1)
-    padded = jnp.concatenate([before, gated], axis=0)
-    convolved = jnp.zeros((tok_rows, channels), jnp.float32) + conv_bias
-    for offset in range(reach_rows + 1):
-        convolved = convolved + padded[offset : offset + tok_rows].astype(jnp.float32) * kernel[
-            offset
-        ].astype(jnp.float32)
-    totals = together((jnp.sum(convolved, axis=1), jnp.sum(convolved * convolved, axis=1)), "tp")
-    average = (totals[0] / full_channels)[:, None]
-    spread = (totals[1] / full_channels)[:, None] - average * average
-    swished = jax.nn.silu((convolved - average) * lax.rsqrt(spread + EPSILON) * ln_gain + ln_bias)
-    energy = of_everyone(jnp.sum(swished * swished, axis=1), "tp")
-    branch = (swished * lax.rsqrt(energy / full_channels + EPSILON)[:, None] * out_gain).astype(
-        jnp.bfloat16
-    )
-    row_count = tok_rows // lax.axis_size("tp")
-    regrouped = lax.all_to_all(branch, "tp", split_axis=0, concat_axis=1, tiled=True)
-    projected = jnp.dot(regrouped, out_weight, preferred_element_type=jnp.float32)
-    hidden = (residual.astype(jnp.float32) + projected).astype(jnp.bfloat16)
-    widened = hidden.astype(jnp.float32)
-    normed = (
-        widened * lax.rsqrt(jnp.mean(widened * widened, axis=1, keepdims=True) + EPSILON) * moe_gain
-    ).astype(jnp.bfloat16)
-    meta = route(expert_ids, expert_weights)
-    cores = jnp.repeat(meta, 2, axis=0)
-    shared = lax.all_to_all(cores, "sp", split_axis=0, concat_axis=0, tiled=True)
-    mine = lax.dynamic_index_in_dim(
-        shared.reshape(PLANES, 2, *meta.shape[1:]), lax.axis_index("sp") % 2, axis=1, keepdims=False
-    )
-    return experts_kernel(hidden, normed, expert_ids, mine, w_gate, w_up, w_down)
+    return experts_kernel(hidden, normed, expert_ids, meta, w_gate, w_up, w_down)
 
 
 def solution(mesh):

time: 254 us -> 221 us (0.87)
  the two profiles are of different devices: /device:TPU:40 before, /device:TPU:168 now
where the time goes in v2:
time: 221 us; the launch traced here: 220 us
  Pallas kernels  206 us (93%)
  local copies, waits for them, and re-layouts  13.6 us (6%)
    pallas_call x1, Pallas kernels, experts_kernel(): pl.pallas_call(moe_body, out_shape=jax.ShapeDtypeStruct((rows, width), BF...  174 us
    pallas_call x1, Pallas kernels, front_kernel(): pl.pallas_call(front_body, out_shape=(jax.ShapeDtypeStruct((rows, width),...  32.4 us
    unnamed x25, local copies, waits for them, and re-layouts  12.9 us

profile of v2, /device:TPU:168, one launch (start us, length us, event | category | flops | bytes accessed | tf_op | source)
XLA Modules:
  0.0 220.1 jit_solution(5082051896720507309)
XLA Ops:
  0.0 0.7 concatenate.3.vec_ref
  0.8 0.8 copy.16.col_ref
  1.5 0.0 copy-start.1
  1.5 0.8 copy.17.load_ref
  2.4 0.0 copy-start
  2.4 2.2 copy-done
  4.5 0.0 copy-start.2
  4.5 1.0 copy-done.2
  5.6 0.0 copy-start.5
  5.6 0.9 copy-done.5
  6.5 0.9 copy-done.6
  7.5 0.0 copy-start.8
  7.5 0.7 copy-done.8
  8.2 0.0 copy-start.9
  8.2 0.7 copy-done.9
  8.9 0.7 copy-done.10
  9.6 32.4 %shard_map.145 = (bf16[128,2048]{1,0:T(8,128)(2,1)S(1)}, bf16[128,2048]{1,0:T(8,128)(2,1)S(1)}, f32[16,8,128]{2,1,0:T(8,128)S(1)}) custom-call(bf16[512,256]{1,0:T(8,128)(2,1)S(1)} %copy-done.5, bf16[512,256]{1,0:T(8,128)(2,1)S(1)} %copy-done.6, bf16[31,256]{1,0:T(8,128)(2,1)S(1)} %copy-done.8, f32[8,256]{1,0:T(8,128)S(1)} %concatenate.3.vec_ref, ...), custom_call_target="tpu_custom_call" | custom-call | tf_op jit(solution)/shard_map/pallas_call | solution.py:625
  42.0 0.0 copy-done.1
  42.0 0.0 copy-start.3
  42.0 0.8 copy-done.3
  42.8 0.8 copy-done.4
  43.6 0.6 copy-done.7
  44.2 174.1 %shard_map.146 = bf16[128,2048]{1,0:T(8,128)(2,1)} custom-call(bf16[128,2048]{1,0:T(8,128)(2,1)} %copy-done.3, bf16[128,2048]{1,0:T(8,128)(2,1)} %copy-done.4, s32[128,2]{1,0:T(8,128)} %copy-done.1, s32[2,128]{1,0:T(2,128)} %bitcast.6, f32[16,8,128]{2,1,0:T(8,128)} %copy-done.7, bf16[1,2048,512]{2,1,0:T(8,128)(2,1)} %wg_hbm.1, bf16[1,2048,512]{2,1,0:T(8,128)(2,1)} %wu_hbm.1, ...), custom_call_target="tpu_custom_call" | custom-call | tf_op jit(solution)/shard_map/pallas_call | solution.py:402
  218.3 1.9 copy.20
  (5 shorter events, 0.0 us)
Async XLA Ops:
  1.5 40.4 %copy-start.1 = (s32[128,2]{1,0:T(8,128)}, s32[128,2]{1,0:T(8,128)S(1)}, u32[]{:S(2)}) copy-start(s32[128,2]{1,0:T(8,128)S(1)} %copy.16.col_ref) | copy-start | bytes 3076
  2.4 2.2 copy-start
  4.5 1.0 copy-start.2
  5.6 0.9 copy-start.5
  6.5 0.9 copy-start.6
  7.5 0.7 copy-start.8
  8.2 0.7 copy-start.9
  8.9 0.7 copy-start.10
  42.0 0.8 copy-start.3
  42.8 0.8 copy-start.4
  43.6 0.6 copy-start.7

commit v3 on v2

--- a/solution.py
+++ b/solution.py
@@ -1,3 +1,5 @@
+import functools
+
 import jax
 import jax.numpy as jnp
 from jax import lax
@@ -16,6 +18,7 @@
 HOPS = 9
 SEATS = 8
 UNIT = 32
+NARROW, WIDE = 48, 64
 BLOCKS = 3 + 2 * (HOPS - 1)
 
 
@@ -71,9 +74,10 @@
     return out
 
 
-def route_body(col_ref, row_ref, wcol_ref, meta_ref, zed):
-    col, row = col_ref[...], row_ref[...]
-    size = col.shape[0]
+def route_tables(row, loads, meta_ref, zed):
+    size = row.shape[1]
+    cols = columns_of(row, loads)
+    col = cols[:, 0:2].astype(jnp.int32)
     zo, g0 = lax.rem(zed, SPAN), lax.div(zed, SPAN)
     r = ranks(col, row)
     e1c, e2c = col[:, 0:1], col[:, 1:2]
@@ -99,14 +103,21 @@
             lane = jnp.where((e >> 3) == plane, (e & 7) * 16 + place[k], -1)
             hit = lane == lanes
             slot_row = slot_row + jnp.sum(jnp.where(hit, slot + 1.0, 0.0), axis=0, keepdims=True)
-            weight_row = weight_row + jnp.sum(jnp.where(hit, wcol_ref[:, k : k + 1], 0.0), axis=0, keepdims=True)
+            weight_row = weight_row + jnp.sum(jnp.where(hit, cols[:, 2 + k : 3 + k], 0.0), axis=0, keepdims=True)
         meta_ref[plane] = jnp.concatenate([slot_row, weight_row, jnp.zeros((6, 128), F32)], axis=0)
+    return jnp.broadcast_to(jnp.where(r["Pr"] >= NARROW, 1.0, 0.0), (8, size))
+
+
+def columns_of(*rows):
+    stack = jnp.concatenate([r.astype(F32) for r in rows], axis=0)
+    stack = jnp.concatenate([stack, jnp.zeros((8 - stack.shape[0], stack.shape[1]), F32)], axis=0)
+    return jnp.transpose(stack, (1, 0))
 
 
 def moe_body(
-    hidden_ref, normed_ref, col_ref, row_ref, meta_ref, wg_hbm, wu_hbm, wd_hbm, out_ref,
-    wg, wu, wd, own, came, back, part, xs, xr, rb, yr,
-    wsem, fsend, frecv, bsend, brecv, xsend, xrecv, ysend, yrecv,
+    cap, normed_hbm, row_hbm, meta_hbm, wg_hbm, wu_hbm, wd_hbm, out_ref,
+    normed_ref, row_ref, meta_ref, wg, wu, wd, own, came, back, part, xs, xr, rb, yr,
+    isem, wsem, fsend, frecv, bsend, brecv, xsend, xrecv, ysend, yrecv,
 ):
     sp, tp = lax.axis_index("sp"), lax.axis_index("tp")
     zed, core = lax.div(sp, 2), lax.rem(sp, 2)
@@ -121,6 +132,14 @@
     def seat_device(s):
         return {"sp": zed * 2 + lax.div(s, 4), "tp": lax.rem(s, 4)}
 
+    small = [
+        pltpu.make_async_copy(row_hbm, row_ref, isem.at[0]),
+        pltpu.make_async_copy(normed_hbm, normed_ref, isem.at[1]),
+        pltpu.make_async_copy(meta_hbm, meta_ref, isem.at[2]),
+    ]
+    for w in small:
+        w.start()
+    pieces = (pl.ds(0, UNIT), pl.ds(UNIT, cap - UNIT))
     weights = [
         pltpu.make_async_copy(wg_hbm.at[0], wg, wsem.at[0]),
         pltpu.make_async_copy(wu_hbm.at[0], wu, wsem.at[1]),
@@ -136,34 +155,37 @@
         @pl.when(off[d] == SPAN - 1)
         def _():
             for hop in range(1, HOPS + 1):
-                came[d, first_block(hop), 1] = jnp.zeros(came.shape[3:], BF16)
+                came[d, first_block(hop), UNIT:cap] = jnp.zeros((cap - UNIT, came.shape[3]), BF16)
 
     barrier = pltpu.get_barrier_semaphore()
     for to in ring_to:
         pl.semaphore_signal(barrier, inc=1, device_id=to, device_id_type=MESH)
     for k in range(1, SEATS):
         pl.semaphore_signal(barrier, inc=1, device_id=seat_device(lax.rem(seat + k, SEATS)), device_id_type=MESH)
-    pl.semaphore_wait(barrier, SEATS + 1)
-
-    r = ranks(col_ref[...], row_ref[...])
+
+    small[0].wait()
+    row = row_ref[...]
+    tokens = row.shape[1]
+    r = ranks(columns_of(row)[:, 0:2].astype(jnp.int32), row)
+    small[1].wait()
     normed = normed_ref[...]
-    tokens = normed.shape[0]
     for d, name in ((0, "P"), (1, "M")):
-        slot = r["gr"] * 64 + r[name + "r"]
-        onehot = jnp.where(iota((GROUPS * 64, tokens), 0) == slot, 1.0, 0.0).astype(BF16)
+        slot = r["gr"] * cap + r[name + "r"]
+        onehot = jnp.where(iota((GROUPS * cap, tokens), 0) == slot, 1.0, 0.0).astype(BF16)
         rows = jnp.dot(onehot, normed, preferred_element_type=F32).astype(BF16)
         own[d] = rows.reshape(own.shape[1:])
+    pl.semaphore_wait(barrier, SEATS + 1)
 
     def forward(d, src, hop, index, unit):
         return pltpu.make_async_remote_copy(
-            src_ref=src, dst_ref=came.at[d, index, unit],
+            src_ref=src, dst_ref=came.at[d, index, pieces[unit]],
             send_sem=fsend.at[d, index, unit], recv_sem=frecv.at[d, index, unit],
             device_id=ring_to[d], device_id_type=MESH,
         )
 
     def backward(d, src, index, unit):
         return pltpu.make_async_remote_copy(
-            src_ref=src, dst_ref=back.at[d, index, unit],
+            src_ref=src, dst_ref=back.at[d, index, pieces[unit]],
             send_sem=bsend.at[d, index, unit], recv_sem=brecv.at[d, index, unit],
             device_id=ring_from[d], device_id_type=MESH,
         )
@@ -180,7 +202,7 @@
 
                     @pl.when(fine)
                     def _():
-                        act(forward(d, own.at[d, group, unit], 1, rel, unit), d, rel, unit)
+                        act(forward(d, own.at[d, group, pieces[unit]], 1, rel, unit), d, rel, unit)
 
     first_hop(lambda copy, *_: copy.start())
 
@@ -206,13 +228,13 @@
     def relay(hop):
         def act(d, rel, unit):
             index = first_block(hop) + rel
-            forward(d, came.at[d, index, unit], hop, index, unit).wait_recv()
+            forward(d, came.at[d, index, pieces[unit]], hop, index, unit).wait_recv()
             if hop < HOPS:
                 ok, there = goes_on(d, hop, rel, unit)
 
                 @pl.when(ok)
                 def _():
-                    forward(d, came.at[d, index, unit], hop + 1, there, unit).start()
+                    forward(d, came.at[d, index, pieces[unit]], hop + 1, there, unit).start()
 
         arrivals(hop, act)
 
@@ -243,7 +265,7 @@
             meta = meta_ref[whose]
             if k:
                 meta = pltpu.roll(meta, 4 * k, 1)
-            slots.append(iota((64, 128), 0).astype(F32) == meta[0:1])
+            slots.append(iota((cap, 128), 0).astype(F32) == meta[0:1])
             loads.append(meta[1:2])
         return slots, loads
 
@@ -254,7 +276,7 @@
         blocks = []
         for source in batches[b]:
             ref = own.at[0, g0] if source is None else came.at[source[0], source[1]]
-            blocks.append(ref[...].reshape(64, ref.shape[-1]))
+            blocks.append(ref[...])
         rows = jnp.dot(pick, jnp.concatenate(blocks, axis=0), preferred_element_type=F32)
         xs[b] = rows.astype(BF16).reshape(xs.shape[1:])
         pltpu.make_async_copy(xs.at[b, seat], xr.at[b, seat], xrecv.at[b]).start()
@@ -297,6 +319,8 @@
         total = jnp.dot(high, rows, preferred_element_type=F32) + jnp.dot(low, rows, preferred_element_type=F32)
         part[b] = total.astype(BF16).reshape(part.shape[1:])
 
+    small[2].wait()
+    tight = cap < WIDE
     relay(1)
     relay(2)
     spread(0)
@@ -305,57 +329,89 @@
     spread(1)
     for w in weights:
         w.wait()
-    expert(0)
+    if tight:
+        expert(0)
     relay(5)
     relay(6)
     spread(2)
-    expert(1)
-    combine(0)
+    if tight:
+        expert(1)
+        combine(0)
     relay(7)
     relay(8)
     relay(9)
     spread(3)
-    expert(2)
-    combine(1)
-    expert(3)
-    combine(2)
-    combine(3)
-
-    def hand_back(hop):
+
+    def early(d, hop, rel):
+        if rel or hop > 6:
+            return None
+        if hop == 6:
+            return off[d] == SPAN - 1
+        return off[d] >= SPAN - 2
+
+    def hand_back(hop, when):
         for rel in reversed(kinds_at(hop)):
             for unit in (0, 1):
                 for d in (0, 1):
                     fine = valid(off[d], hop, rel)
                     if unit == 1 and rel == 0:
                         fine = fine & (off[d] < SPAN - 1)
+                    ahead = early(d, hop, rel)
+                    if when == "end":
+                        if ahead is None or unit == 1:
+                            continue
+                        fine = fine & (off[d] == SPAN - 1)
+                    elif when == "middle":
+                        if ahead is None or hop == 6:
+                            continue
+                        fine = fine & (off[d] == SPAN - 2)
+                    elif when == "rest" and ahead is not None:
+                        fine = fine & jnp.logical_not(ahead)
                     index = first_block(hop) + rel
                     b, k = where_part(d, hop) if rel == 0 else (0, 0)
 
                     @pl.when(fine)
                     def _():
                         if rel == 0:
-                            if hop < HOPS:
+                            if hop < HOPS and when != "end":
                                 later = first_block(hop + 1)
 
                                 @pl.when(off[d] < SPAN - 1 - unit)
                                 def _():
-                                    backward(d, back.at[d, later, unit], later, unit).wait_recv()
-                                    part[b, k, unit] = (
-                                        part[b, k, unit].astype(F32) + back[d, later, unit].astype(F32)
+                                    backward(d, back.at[d, later, pieces[unit]], later, unit).wait_recv()
+                                    part[b, k, pieces[unit]] = (
+                                        part[b, k, pieces[unit]].astype(F32) + back[d, later, pieces[unit]].astype(F32)
                                     ).astype(BF16)
 
-                            backward(d, part.at[b, k, unit], index, unit).start()
+                            backward(d, part.at[b, k, pieces[unit]], index, unit).start()
                         else:
                             later = first_block(hop + 1) + rel - last[d]
-                            backward(d, back.at[d, later, unit], later, unit).wait_recv()
-                            backward(d, back.at[d, later, unit], index, unit).start()
-
+                            backward(d, back.at[d, later, pieces[unit]], later, unit).wait_recv()
+                            backward(d, back.at[d, later, pieces[unit]], index, unit).start()
+
+    if tight:
+        expert(2)
+        combine(1)
+        combine(2)
+        for hop in range(6, 0, -1):
+            hand_back(hop, "end")
+        expert(3)
+        for hop in range(5, 0, -1):
+            hand_back(hop, "middle")
+    else:
+
+        @pl.loop(0, len(batches))
+        def _(b):
+            expert(b)
+
+        for b in range(len(batches) - 1):
+            combine(b)
+    combine(3)
     for hop in range(HOPS, 0, -1):
-        hand_back(hop)
-
-    first_hop(lambda copy, d, rel, unit: backward(d, back.at[d, rel, unit], rel, unit).wait_recv())
+        hand_back(hop, "rest" if tight else "all")
+
+    first_hop(lambda copy, d, rel, unit: backward(d, back.at[d, rel, pieces[unit]], rel, unit).wait_recv())
     group, up_rank, down_rank = r["gc"], r["Pc"], r["Mc"]
-    lanes = iota((tokens, 64), 1)
     far = jnp.where(zo >= 2, 0, 1)
     far_rank = jnp.where(zo >= 2, up_rank, down_rank)
     plan = [
@@ -366,11 +422,12 @@
         (group == lax.rem(g0 + 2, GROUPS), far_rank, back.at[far, 2 - jnp.where(zo >= 2, last[0], last[1])]),
         (group == g0, up_rank, part.at[3, 0]),
     ]
-    pick = [jnp.where((jnp.where(mask, rank, -1) == lanes), 1.0, 0.0) for mask, rank, _ in plan]
-    pick = jnp.concatenate(pick, axis=1).astype(BF16)
-    blocks = jnp.concatenate([ref[...].reshape(64, ref.shape[-1]) for _, _, ref in plan], axis=0)
-    total = jnp.dot(pick, blocks, preferred_element_type=F32)
-    out_ref[...] = (hidden_ref[...].astype(F32) + total).astype(BF16)
+    lanes = iota((tokens, len(plan) * cap), 1)
+    pick = jnp.zeros(lanes.shape, F32)
+    for i, (mask, rank, _) in enumerate(plan):
+        pick = pick + jnp.where(jnp.where(mask, rank + i * cap, -1) == lanes, 1.0, 0.0)
+    blocks = jnp.concatenate([ref[...] for _, _, ref in plan], axis=0)
+    out_ref[...] = jnp.dot(pick.astype(BF16), blocks, preferred_element_type=F32)
 
     first_hop(lambda copy, *_: copy.wait_send())
     for hop in range(1, HOPS + 1):
@@ -381,9 +438,9 @@
 
                 @pl.when(ok)
                 def _():
-                    forward(d, came.at[d, index, unit], hop + 1, there, unit).wait_send()
-
-            backward(d, back.at[d, index, unit], index, unit).wait_send()
+                    forward(d, came.at[d, index, pieces[unit]], hop + 1, there, unit).wait_send()
+
+            backward(d, back.at[d, index, pieces[unit]], index, unit).wait_send()
 
         arrivals(hop, done)
     for b in range(len(batches)):
@@ -392,42 +449,46 @@
             return_copy(b, k).wait_send()
 
 
-def experts_kernel(hidden, normed, ids, meta, w_gate, w_up, w_down):
+def experts_kernel(cap, normed, ids, meta, w_gate, w_up, w_down):
     rows, width = normed.shape
     inner = w_gate.shape[2]
-    vmem = pl.BlockSpec(memory_space=pltpu.VMEM)
-    far = pl.BlockSpec(memory_space=pl.ANY)
+    far = pl.BlockSpec(memory_space=pltpu.HBM)
     seats = pltpu.VMEM((4, SEATS, 16, width), BF16)
     dma = pltpu.SemaphoreType.DMA
     return pl.pallas_call(
-        moe_body,
-        out_shape=jax.ShapeDtypeStruct((rows, width), BF16),
-        in_specs=[vmem] * 5 + [far] * 3,
-        out_specs=vmem,
+        functools.partial(moe_body, cap),
+        out_shape=jax.ShapeDtypeStruct((rows, width), F32),
+        in_specs=[far] * 6,
+        out_specs=pl.BlockSpec(memory_space=pltpu.VMEM),
         scratch_shapes=[
+            pltpu.VMEM((rows, width), BF16),
+            pltpu.VMEM(ids.shape, jnp.int32),
+            pltpu.VMEM(meta.shape, F32),
             pltpu.VMEM((width, inner), BF16),
             pltpu.VMEM((width, inner), BF16),
             pltpu.VMEM((inner, width), BF16),
-            pltpu.VMEM((2, GROUPS, 2, UNIT, width), BF16),
-            pltpu.VMEM((2, BLOCKS, 2, UNIT, width), BF16),
-            pltpu.VMEM((2, BLOCKS, 2, UNIT, width), BF16),
-            pltpu.VMEM((4, 4, 2, UNIT, width), BF16),
+            pltpu.VMEM((2, GROUPS, cap, width), BF16),
+            pltpu.VMEM((2, BLOCKS, cap, width), BF16),
+            pltpu.VMEM((2, BLOCKS, cap, width), BF16),
+            pltpu.VMEM((4, 4, cap, width), BF16),
             seats, seats, seats, seats,
-            dma((3,)),
+            dma((3,)), dma((3,)),
             dma((2, BLOCKS, 2)), dma((2, BLOCKS, 2)), dma((2, BLOCKS, 2)), dma((2, BLOCKS, 2)),
             dma((4, SEATS)), dma((4,)), dma((4, SEATS)), dma((4,)),
         ],
         compiler_params=pltpu.CompilerParams(
-            collective_id=1, has_side_effects=True, vmem_limit_bytes=60 << 20
+            collective_id=1 if cap == WIDE else 3, has_side_effects=True, vmem_limit_bytes=60 << 20
         ),
-    )(hidden, normed, ids, ids.T, meta, w_gate, w_up, w_down)
+    )(normed, ids, meta, w_gate, w_up, w_down)
 
 
 def front_body(
-    value_ref, gate_ref, taps_ref, vec_ref, gain_ref, col_ref, row_ref, load_ref, weight_hbm, residual_hbm,
-    hidden_ref, normed_ref, meta_ref,
-    weight, residual, gated, grown, packs, conv, tables,
-    lsem, gsend, grecv, hsend, hrecv, psend, precv, tsend, trecv,
+    value_hbm, gate_hbm, taps_hbm, bias_hbm, scale_hbm, shift_hbm, branch_hbm, gain_hbm, row_hbm, load_hbm,
+    weight_hbm, residual_hbm,
+    hidden_ref, normed_ref, meta_ref, crowd_ref,
+    value_ref, gate_ref, taps_ref, vectors, gain_ref, row_ref, load_ref, weight, residual, gated, grown, packs, conv,
+    tables, flags, heard,
+    lsem, csend, crecv, gsend, grecv, hsend, hrecv, psend, precv, tsend, trecv,
 ):
     sp, tp = lax.axis_index("sp"), lax.axis_index("tp")
     steps, teams = lax.axis_size("sp"), lax.axis_size("tp")
@@ -435,6 +496,21 @@
     rows = hidden_ref.shape[0]
     pieces = rows // UNIT
     channels = value_ref.shape[1]
+    parts = lax.axis_size("grp")
+    other = zed * 2 + 1 - core
+    loads = [
+        (row_hbm, row_ref), (load_hbm, load_ref),
+        (value_hbm, value_ref), (gate_hbm, gate_ref), (taps_hbm, taps_ref),
+        (bias_hbm, vectors.at[0]), (scale_hbm, vectors.at[1]), (shift_hbm, vectors.at[2]), (branch_hbm, vectors.at[3]),
+        (residual_hbm, residual), (gain_hbm, gain_ref), (weight_hbm, weight),
+    ]
+    copies = [pltpu.make_async_copy(a, b, lsem.at[i]) for i, (a, b) in enumerate(loads)]
+    for copy in copies:
+        copy.start()
+    fetch, first, late = copies[:2], copies[2:9], copies[9:]
+
+    def part_of(k):
+        return lax.rem(lax.axis_index("grp") + k, parts)
 
     def team(k):
         return lax.rem(tp + k, teams)
@@ -453,23 +529,28 @@
 
     for k in range(1, PLANES):
         pl.semaphore_signal(barrier, inc=1, device_id={"sp": column(k)}, device_id_type=MESH)
-
-    fetch_weight = pltpu.make_async_copy(weight_hbm, weight, lsem.at[0])
-    fetch_residual = pltpu.make_async_copy(residual_hbm, residual, lsem.at[1])
-    fetch_weight.start()
-    fetch_residual.start()
-
+    for k in range(teams):
+        pl.semaphore_signal(barrier, inc=1, device_id={"sp": other, "tp": k}, device_id_type=MESH)
+    for k in range(1, parts):
+        pl.semaphore_signal(barrier, inc=1, device_id={"grp": part_of(k)}, device_id_type=MESH)
+
+    for copy in fetch:
+        copy.wait()
+    crowd = route_tables(row_ref[...], load_ref[...], tables, zed)
+    flags[0] = crowd
+    for copy in first:
+        copy.wait()
     passed = (value_ref[...].astype(F32) * jax.nn.sigmoid(gate_ref[...].astype(F32))).astype(BF16)
     gated[...] = passed.reshape(gated.shape)
     packs[tp, 0 : taps_ref.shape[0]] = taps_ref[...].astype(F32)
-    packs[tp, 32:40] = vec_ref[...]
+    for i in range(4):
+        packs[tp, 32 + i : 33 + i] = vectors[i]
 
     @pl.when((sp == 0) & (tp == 0))
     def _():
         grown[:, 0] = jnp.zeros((teams, UNIT, channels), BF16)
 
-    route_body(col_ref, row_ref, load_ref, tables, zed)
-    pl.semaphore_wait(barrier, teams + PLANES - 2 + jnp.where(sp < steps - 1, 1, 0))
+    pl.semaphore_wait(barrier, 2 * teams + PLANES + parts - 3 + jnp.where(sp < steps - 1, 1, 0))
 
     def whole(to, k):
         return pltpu.make_async_remote_copy(
@@ -526,6 +607,45 @@
 
     for k in range(1, PLANES):
         table_copy(k).start()
+
+    plane_mates = [{"tp": team(k)} for k in range(1, teams)] + [{"sp": other, "tp": k} for k in range(teams)]
+    rounds = [
+        [(to, i) for i, to in enumerate(plane_mates)],
+        [({"grp": part_of(k)}, k) for k in range(1, parts)],
+        [({"sp": column(k)}, k) for k in range(1, PLANES)],
+    ]
+
+    def flag_copies(stage):
+        base = (0, 16, 16 + parts)[stage]
+        return [
+            pltpu.make_async_remote_copy(
+                src_ref=flags.at[stage], dst_ref=heard.at[land(stage, base, i)], send_sem=csend.at[base + i],
+                recv_sem=crecv.at[land(stage, base, i)], device_id=to, device_id_type=MESH,
+            )
+            for to, i in rounds[stage]
+        ]
+
+    def land(stage, base, i):
+        if stage == 0 and i >= teams - 1:
+            return base + teams - 1 + tp
+        return base + i
+
+    def hear(stage):
+        base = (0, 16, 16 + parts)[stage]
+        seen = flags[stage]
+        for (to, i) in rounds[stage]:
+            pltpu.make_async_remote_copy(
+                src_ref=flags.at[stage], dst_ref=heard.at[base + i], send_sem=csend.at[base + i],
+                recv_sem=crecv.at[base + i], device_id=to, device_id_type=MESH,
+            ).wait_recv()
+            seen = jnp.maximum(seen, heard[base + i])
+        flags[stage + 1] = seen
+        if stage < 2:
+            for copy in flag_copies(stage + 1):
+                copy.start()
+
+    for copy in flag_copies(0):
+        copy.start()
 
     for test, size in ((tp == 0, 0), (tp > 0, 1)):
 
@@ -556,6 +676,8 @@
     shift0 = UNIT - reach
     for k in (0, 1, 3, 2):
         wait_part(k)
+        if k in (1, 2):
+            hear(0 if k == 1 else 1)
         source = team(k)
         for half in range(channels // 128):
             lanes = pl.ds(half * 128, 128)
@@ -574,9 +696,9 @@
             conv[source, :, lanes] = total
 
     full = channels * teams
-    parts = [conv[s] for s in range(teams)]
-    average = sum(jnp.sum(p, axis=1, keepdims=True) for p in parts) / full
-    spread = sum(jnp.sum(p * p, axis=1, keepdims=True) for p in parts) / full - average * average
+    pieces_of = [conv[s] for s in range(teams)]
+    average = sum(jnp.sum(p, axis=1, keepdims=True) for p in pieces_of) / full
+    spread = sum(jnp.sum(p * p, axis=1, keepdims=True) for p in pieces_of) / full - average * average
     scale = lax.rsqrt(spread + EPSILON)
     energy = jnp.zeros((rows, 1), F32)
     for s in range(teams):
@@ -585,8 +707,8 @@
         energy = energy + jnp.sum(v * v, axis=1, keepdims=True)
     scale = lax.rsqrt(energy / full + EPSILON)
     branch = jnp.concatenate([(conv[s] * scale * packs[s, 35:36]).astype(BF16) for s in range(teams)], axis=1)
-    fetch_weight.wait()
-    fetch_residual.wait()
+    for copy in late:
+        copy.wait()
     projected = jnp.dot(branch, weight[...], preferred_element_type=F32)
     hidden = (residual[...].astype(F32) + projected).astype(BF16)
     hidden_ref[...] = hidden
@@ -599,6 +721,12 @@
         table_copy(k).wait_recv()
         meta_ref[lax.rem(zed + PLANES - k, PLANES)] = tables[PLANES + k]
 
+    hear(2)
+    crowd_ref[0] = jnp.max(flags[3]).astype(jnp.int32)
+    for stage in range(3):
+        for copy in flag_copies(stage):
+            copy.wait_send()
+
     for k in range(1, teams):
         pack_copy(k).wait_send()
         for test, copy in ((team(k) == 0, short), (team(k) > 0, whole)):
@@ -620,18 +748,27 @@
     tok_rows, channels = value.shape
     teams = lax.axis_size("tp")
     vmem = pl.BlockSpec(memory_space=pltpu.VMEM)
-    far = pl.BlockSpec(memory_space=pl.ANY)
+    far = pl.BlockSpec(memory_space=pltpu.HBM)
     dma = pltpu.SemaphoreType.DMA
+    voices = 16 + lax.axis_size("grp") + PLANES
     return pl.pallas_call(
         front_body,
         out_shape=(
             jax.ShapeDtypeStruct((rows, width), BF16),
             jax.ShapeDtypeStruct((rows, width), BF16),
             jax.ShapeDtypeStruct((PLANES, 8, 128), F32),
+            jax.ShapeDtypeStruct((1,), jnp.int32),
         ),
-        in_specs=[vmem] * 8 + [far] * 2,
-        out_specs=[vmem] * 3,
+        in_specs=[far] * 12,
+        out_specs=[vmem] * 3 + [pl.BlockSpec(memory_space=pltpu.SMEM)],
         scratch_shapes=[
+            pltpu.VMEM(value.shape, BF16),
+            pltpu.VMEM(value.shape, BF16),
+            pltpu.VMEM(taps.shape, BF16),
+            pltpu.VMEM((4, 1, channels), F32),
+            pltpu.VMEM(moe_gain.shape, F32),
+            pltpu.VMEM(ids.shape, jnp.int32),
+            pltpu.VMEM(loads.shape, F32),
             pltpu.VMEM(out_weight.shape, BF16),
             pltpu.VMEM((rows, width), BF16),
             pltpu.VMEM((tok_rows // UNIT, UNIT, channels), BF16),
@@ -639,13 +776,16 @@
             pltpu.VMEM((teams, 40, channels), F32),
             pltpu.VMEM((teams, rows, channels), F32),
             pltpu.VMEM((2 * PLANES, 8, 128), F32),
-            dma((2,)), dma((teams,)), dma((teams,)), dma((1,)), dma((teams,)), dma((teams,)), dma((teams,)),
+            pltpu.VMEM((4, 8, 128), F32),
+            pltpu.VMEM((voices, 8, 128), F32),
+            dma((12,)), dma((voices,)), dma((voices,)),
+            dma((teams,)), dma((teams,)), dma((1,)), dma((teams,)), dma((teams,)), dma((teams,)),
             dma((PLANES,)), dma((PLANES,)),
         ],
         compiler_params=pltpu.CompilerParams(
-            collective_id=2, has_side_effects=True, vmem_limit_bytes=40 << 20
+            collective_id=2, has_side_effects=True, vmem_limit_bytes=60 << 20
         ),
-    )(value, gate, taps, vectors, moe_gain, ids, ids.T, loads, out_weight, residual)
+    )(value, gate, taps, *vectors, moe_gain, ids, loads, out_weight, residual)
 
 
 def per_device(
@@ -665,12 +805,18 @@
     w_up,
     w_down,
 ):
-    nothing = jnp.zeros((4, conv_bias.shape[0]), jnp.float32)
-    vectors = jnp.concatenate([jnp.stack([conv_bias, ln_gain, ln_bias, out_gain]), nothing], axis=0)
-    hidden, normed, meta = front_kernel(
-        conv_value, conv_gate, kernel, vectors, moe_gain[None], expert_ids, expert_weights, out_weight, residual
+    ids = expert_ids.T
+    vectors = [v[None] for v in (conv_bias, ln_gain, ln_bias, out_gain)]
+    hidden, normed, meta, crowd = front_kernel(
+        conv_value, conv_gate, kernel, vectors, moe_gain[None], ids, expert_weights.T, out_weight, residual
     )
-    return experts_kernel(hidden, normed, expert_ids, meta, w_gate, w_up, w_down)
+    added = lax.cond(
+        crowd[0] > 0,
+        functools.partial(experts_kernel, WIDE),
+        functools.partial(experts_kernel, NARROW),
+        normed, ids, meta, w_gate, w_up, w_down,
+    )
+    return (hidden.astype(F32) + added).astype(BF16)
 
 
 def solution(mesh):

time: 221 us -> 203 us (0.919)
  the two profiles are of different devices: /device:TPU:168 before, /device:TPU:40 now
where the time goes in v3:
time: 203 us
  Pallas kernels  200 us (99%)
    pallas_call x1, Pallas kernels, experts_kernel(): pl.pallas_call(functools.partial(moe_body, cap), out_shape=jax.ShapeDtype...  154 us
    pallas_call x1, Pallas kernels, front_kernel(): pl.pallas_call(front_body, out_shape=(jax.ShapeDtypeStruct((rows, width),...  46.1 us

profile of v3, /device:TPU:40, one launch (start us, length us, event | category | flops | bytes accessed | tf_op | source)
XLA Modules:
  0.0 202.9 jit_solution(3012413592682888251)
XLA Ops:
  0.0 0.0 copy-start
  0.0 0.0 copy-start.1
  0.0 46.1 %shard_map.145 = (bf16[128,2048]{1,0:T(8,128)(2,1)}, bf16[128,2048]{1,0:T(8,128)(2,1)S(1)}, f32[16,8,128]{2,1,0:T(8,128)S(1)}, s32[1]{0:T(128)}) custom-call(bf16[512,256]{1,0:T(8,128)(2,1)} %value_hbm.1, bf16[512,256]{1,0:T(8,128)(2,1)} %gate_hbm.1, bf16[31,256]{1,0:T(8,128)(2,1)} %taps_hbm.1, f32[1,256]{1,0:T(1,128)} %bitcast.12, f32[1,256]{1,0:T(1,128)} %bitcast.13, ...), custom_call_target="tpu_custom_call" | custom-call | tf_op jit(solution)/shard_map/pallas_call | solution.py:754
  46.8 0.0 copy-done
  46.8 0.0 copy-done.1
  46.8 154.1 %conditional.1 = (f32[128,2048]{1,0:T(8,128)S(1)}) conditional(s32[]{:T(128)} %bitcast.7, (bf16[128,2048]{1,0:T(8,128)(2,1)S(1)}, s32[2,128]{1,0:T(2,128)S(1)}, f32[16,8,128]{2,1,0:T(8,128)S(1)}, bf16[1,2048,512]{2,1,0:T(8,128)(2,1)S(1)}, bf16[1,2048,512]{2,1,0:T(8,128)(2,1)}, /*index=5*/bf16[1,512,2048]{2,1,0:T(8,128)(2,1)}) %tuple.16, ...), branch_computations={%region_0.0_spmd, %region_1.0_spmd} | conditional | bytes 8 | solution.py:813
  46.8 153.9 %branch_0_fun.1 = f32[128,2048]{1,0:T(8,128)S(1)} custom-call(bf16[128,2048]{1,0:T(8,128)(2,1)S(1)} %get-tuple-element.32.normed_hbm, s32[2,128]{1,0:T(2,128)S(1)} %get-tuple-element.33.row_hbm, f32[16,8,128]{2,1,0:T(8,128)S(1)} %get-tuple-element.34.meta_hbm, bf16[1,2048,512]{2,1,0:T(8,128)(2,1)S(1)} %get-tuple-element.35.wg_hbm, ...), custom_call_target="tpu_custom_call" | custom-call | tf_op jit(solution)/shard_map/cond/branch_0_fun/pallas_call | solution.py:458
  201.0 1.9 add_convert_fusion
Async XLA Ops:
  0.0 46.8 %copy-start = (bf16[1,2048,512]{2,1,0:T(8,128)(2,1)S(1)}, bf16[1,2048,512]{2,1,0:T(8,128)(2,1)}, u32[]{:S(2)}) copy-start(bf16[1,2048,512]{2,1,0:T(8,128)(2,1)} %param.29) | copy-start | bytes 6291460
  0.0 46.8 %copy-start.1 = (s32[128,2]{0,1:T(2,128)S(1)}, s32[128,2]{0,1:T(2,128)}, u32[]{:S(2)}) copy-start(s32[128,2]{0,1:T(2,128)} %param.27) | copy-start | bytes 3076

commit v4 on v3

--- a/solution.py
+++ b/solution.py
@@ -20,6 +20,24 @@
 UNIT = 32
 NARROW, WIDE = 48, 64
 BLOCKS = 3 + 2 * (HOPS - 1)
+BATCHES = 8
+FAR = (
+    ((1, 7), (0, 7), (0, 7), (0, 7)),
+    ((1, 8), (1, 7), (1, 7), (0, 8)),
+    ((1, 9), (1, 8), (0, 8), (0, 9)),
+)
+ORDER = (
+    ("r", 1), ("s", 0), ("r", 2), ("s", 1), ("e", 0), ("r", 3), ("s", 2), ("e", 1),
+    ("r", 4), ("s", 3), ("e", 2), ("r", 5), ("s", 4), ("e", 3), ("c", 2), ("r", 6),
+    ("s", 5), ("e", 4), ("r", 7), ("c", 3), ("e", 5), ("w", 0, 4), ("r", 8), ("s", 6),
+    ("c", 4), ("w", 0, 5), ("w", 0, 3), ("r", 9), ("s", 7), ("w", 1, 4), ("c", 5), ("e", 6),
+    ("w", 0, 6), ("w", 1, 5), ("e", 7), ("c", 1), ("w", 0, 2), ("w", 2, 4), ("w", 1, 6), ("c", 6),
+    ("w", 1, 3), ("w", 2, 6), ("c", 7), ("w", 2, 5), ("w", 0, 9), ("w", 0, 8), ("w", 1, 9), ("w", 1, 8),
+    ("c", 0), ("w", 0, 7), ("w", 3, 6), ("w", 2, 9), ("w", 3, 5), ("w", 1, 7), ("w", 1, 2), ("w", 2, 8),
+    ("w", 2, 7), ("w", 4, 6), ("w", 3, 9), ("w", 3, 8), ("w", 2, 3), ("w", 4, 9), ("w", 3, 7), ("w", 5, 9),
+    ("w", 4, 8), ("w", 5, 8), ("w", 6, 9), ("w", 3, 4), ("w", 4, 7), ("w", 0, 1), ("w", 4, 5), ("w", 6, 8),
+    ("w", 5, 7), ("w", 7, 9), ("w", 5, 6), ("w", 7, 8), ("w", 8, 9), ("w", 6, 7),
+)
 
 
 def first_block(hop):
@@ -40,6 +58,17 @@
     start = (on - hop) % SPAN
     kind = (start + hop) // SPAN + rel
     return kind <= 1 or (kind == 2 and start >= 2)
+
+
+def real(wave, end):
+    hop, rel = end - wave, wave // SPAN
+    return (rel < 2 or hop == 1) and static_valid(SPAN - 1 - wave % SPAN, hop, rel)
+
+
+def where_part(d, hop, place):
+    if hop <= 6:
+        return hop - 1, d
+    return ((6, 1), (7, 0), (7, 1))[[FAR[i][place] for i in range(3)].index((d, hop))]
 
 
 def valid(on, hop, rel):
@@ -100,7 +129,7 @@
             own_up = jnp.where(po >= zo, 1, 0)
             up = jnp.where(ahead == 0, own_up, jnp.where(ahead == 1, 1, jnp.where(ahead == 2, far_up, 0)))
             slot = jnp.where(up == 1, r["Pc"], r["Mc"]).astype(F32)
-            lane = jnp.where((e >> 3) == plane, (e & 7) * 16 + place[k], -1)
+            lane = jnp.where((e >> 3) == plane, (e & 7) * 8 + place[k], -1)
             hit = lane == lanes
             slot_row = slot_row + jnp.sum(jnp.where(hit, slot + 1.0, 0.0), axis=0, keepdims=True)
             weight_row = weight_row + jnp.sum(jnp.where(hit, cols[:, 2 + k : 3 + k], 0.0), axis=0, keepdims=True)
@@ -116,7 +145,7 @@
 
 def moe_body(
     cap, normed_hbm, row_hbm, meta_hbm, wg_hbm, wu_hbm, wd_hbm, out_ref,
-    normed_ref, row_ref, meta_ref, wg, wu, wd, own, came, back, part, xs, xr, rb, yr,
+    normed_ref, row_ref, meta_ref, wg, wu, wd, active, own, came, back, part, xs, xr, rb, yr,
     isem, wsem, fsend, frecv, bsend, brecv, xsend, xrecv, ysend, yrecv,
 ):
     sp, tp = lax.axis_index("sp"), lax.axis_index("tp")
@@ -168,12 +197,16 @@
     tokens = row.shape[1]
     r = ranks(columns_of(row)[:, 0:2].astype(jnp.int32), row)
     small[1].wait()
-    normed = normed_ref[...]
     for d, name in ((0, "P"), (1, "M")):
         slot = r["gr"] * cap + r[name + "r"]
         onehot = jnp.where(iota((GROUPS * cap, tokens), 0) == slot, 1.0, 0.0).astype(BF16)
-        rows = jnp.dot(onehot, normed, preferred_element_type=F32).astype(BF16)
-        own[d] = rows.reshape(own.shape[1:])
+
+        @pl.loop(0, own.shape[-1] // 512)
+        def _(i):
+            cols = pl.ds(pl.multiple_of(i * 512, 512), 512)
+            rows = jnp.dot(onehot, normed_ref[:, cols], preferred_element_type=F32).astype(BF16)
+            own[d, :, :, cols] = rows.reshape(GROUPS, cap, 512)
+
     pl.semaphore_wait(barrier, SEATS + 1)
 
     def forward(d, src, hop, index, unit):
@@ -238,47 +271,49 @@
 
         arrivals(hop, act)
 
-    def up_if(flag, a, b):
-        return (jnp.where(flag, a[0], b[0]), jnp.where(flag, first_block(a[1]), first_block(b[1])),
-                jnp.where(flag, zed - a[1], zed + b[1]))
-
-    def fixed(d, hop):
-        return (d, first_block(hop), zed - hop if d == 0 else zed + hop)
-
-    batches = [[fixed(0, h), fixed(1, h), fixed(0, h + 1), fixed(1, h + 1)] for h in (1, 3, 5)]
-    batches.append([
-        None,
-        up_if(zo != 0, (0, 7), (1, 9)),
-        up_if(zo >= 2, (0, 8), (1, 8)),
-        up_if(zo == 3, (0, 9), (1, 7)),
-    ])
-
-    def where_part(d, hop):
-        if hop <= 6:
-            return (hop - 1) // 2, ((hop - 1) % 2) * 2 + d
-        return 3, {(0, 7): 1, (1, 9): 1, (0, 8): 2, (1, 8): 2, (1, 7): 3, (0, 9): 3}[(d, hop)]
+    def near(b):
+        hop = b + 1
+        index = jnp.where(b == 0, 0, 2 * b + 1)
+        return [(0, index, zed + PLANES - hop), (1, index, zed + hop)]
+
+    def by_place(options):
+        out = []
+        for values in zip(*[(d, first_block(h), PLANES - h if d == 0 else h) for d, h in options]):
+            pick = jnp.int32(values[0])
+            for i in range(1, SPAN):
+                pick = jnp.where(zo == i, values[i], pick)
+            out.append(pick)
+        return out[0], out[1], zed + out[2]
+
+    def sources(b):
+        if isinstance(b, int) and b >= 6:
+            return ([None] if b == 6 else []) + [by_place(FAR[i]) for i in ((0,) if b == 6 else (1, 2))]
+        return near(b)
 
     def selectors(b):
         slots, loads = [], []
-        for k, source in enumerate(batches[b]):
-            whose = zed if source is None else lax.rem(source[2] + PLANES, PLANES)
+        for k, source in enumerate(sources(b)):
+            whose = zed if source is None else lax.rem(source[2], PLANES)
             meta = meta_ref[whose]
             if k:
                 meta = pltpu.roll(meta, 4 * k, 1)
-            slots.append(iota((cap, 128), 0).astype(F32) == meta[0:1])
-            loads.append(meta[1:2])
+            slots.append(iota((cap, SEATS * 8), 0).astype(F32) == meta[0:1, 0 : SEATS * 8])
+            loads.append(meta[1:2, 0 : SEATS * 8])
         return slots, loads
 
     def spread(b):
         slots, _ = selectors(b)
         pick = jnp.concatenate([jnp.where(s, 1.0, 0.0) for s in slots], axis=0)
         pick = jnp.transpose(pick, (1, 0)).astype(BF16)
-        blocks = []
-        for source in batches[b]:
-            ref = own.at[0, g0] if source is None else came.at[source[0], source[1]]
-            blocks.append(ref[...])
-        rows = jnp.dot(pick, jnp.concatenate(blocks, axis=0), preferred_element_type=F32)
-        xs[b] = rows.astype(BF16).reshape(xs.shape[1:])
+        refs = [own.at[0, g0] if source is None else came.at[source[0], source[1]] for source in sources(b)]
+
+        @pl.loop(0, xs.shape[-1] // 512)
+        def _(i):
+            cols = pl.ds(pl.multiple_of(i * 512, 512), 512)
+            blocks = jnp.concatenate([ref[:, cols] for ref in refs], axis=0)
+            rows = jnp.dot(pick, blocks, preferred_element_type=F32).astype(BF16)
+            xs[b, :, :, cols] = rows.reshape(SEATS, 8, 512)
+
         pltpu.make_async_copy(xs.at[b, seat], xr.at[b, seat], xrecv.at[b]).start()
         for k in range(1, SEATS):
             spread_copy(b, k).start()
@@ -299,12 +334,21 @@
 
     def expert(b):
         pltpu.make_async_copy(xs.at[b], xr.at[b], xrecv.at[b]).wait()
-        rows = xr[b].reshape(SEATS * 16, xr.shape[-1])
-        gate = jnp.dot(rows, wg[...], preferred_element_type=F32)
-        up = jnp.dot(rows, wu[...], preferred_element_type=F32)
-        active = (jax.nn.silu(gate) * up).astype(BF16)
-        result = jnp.dot(active, wd[...], preferred_element_type=F32).astype(BF16)
-        rb[b] = result.reshape(rb.shape[1:])
+        rows = xr[b].reshape(SEATS * 8, xr.shape[-1])
+
+        @pl.loop(0, wg.shape[1] // 256)
+        def _(i):
+            cols = pl.ds(pl.multiple_of(i * 256, 256), 256)
+            gate = jnp.dot(rows, wg[:, cols], preferred_element_type=F32)
+            up = jnp.dot(rows, wu[:, cols], preferred_element_type=F32)
+            active[:, cols] = (jax.nn.silu(gate) * up).astype(BF16)
+
+        @pl.loop(0, wd.shape[1] // 512)
+        def _(i):
+            cols = pl.ds(pl.multiple_of(i * 512, 512), 512)
+            result = jnp.dot(active[...], wd[:, cols], preferred_element_type=F32).astype(BF16)
+            rb[b, :, :, cols] = result.reshape(SEATS, 8, 512)
+
         pltpu.make_async_copy(rb.at[b, seat], yr.at[b, seat], yrecv.at[b]).start()
         for k in range(1, SEATS):
             return_copy(b, k).start()
@@ -312,103 +356,66 @@
     def combine(b):
         slots, loads = selectors(b)
         pltpu.make_async_copy(rb.at[b], yr.at[b], yrecv.at[b]).wait()
-        rows = yr[b].reshape(SEATS * 16, yr.shape[-1])
         scale = jnp.concatenate([jnp.where(s, w, 0.0) for s, w in zip(slots, loads)], axis=0)
         high = scale.astype(BF16)
         low = (scale - high.astype(F32)).astype(BF16)
-        total = jnp.dot(high, rows, preferred_element_type=F32) + jnp.dot(low, rows, preferred_element_type=F32)
-        part[b] = total.astype(BF16).reshape(part.shape[1:])
+
+        @pl.loop(0, yr.shape[-1] // 512)
+        def _(i):
+            cols = pl.ds(pl.multiple_of(i * 512, 512), 512)
+            rows = yr[b, :, :, cols].reshape(SEATS * 8, 512)
+            total = jnp.dot(high, rows, preferred_element_type=F32) + jnp.dot(low, rows, preferred_element_type=F32)
+            part[b, :, :, cols] = total.astype(BF16).reshape(2, cap, 512)
+
+    def item(wave, end):
+        hop, rel, place = end - wave, wave // SPAN, SPAN - 1 - wave % SPAN
+        for d in (0, 1):
+
+            @pl.when(off[d] == place)
+            def _():
+                index = first_block(hop) + rel
+                for unit in (0, 1):
+                    if rel:
+                        later = first_block(hop + 1) + rel - (place == SPAN - 1)
+                        backward(d, back.at[d, later, pieces[unit]], later, unit).wait_recv()
+                        backward(d, back.at[d, later, pieces[unit]], index, unit).start()
+                    elif unit == 0 or place < SPAN - 1:
+                        b, k = where_part(d, hop, place if d == 0 else SPAN - 1 - place)
+                        mine = part.at[b, k, pieces[unit]]
+                        if place < SPAN - 1 - unit:
+                            later = first_block(hop + 1)
+                            far = back.at[d, later, pieces[unit]]
+                            backward(d, far, later, unit).wait_recv()
+                            mine[...] = (mine[...].astype(F32) + far[...].astype(F32)).astype(BF16)
+                        backward(d, mine, index, unit).start()
 
     small[2].wait()
-    tight = cap < WIDE
-    relay(1)
-    relay(2)
-    spread(0)
-    relay(3)
-    relay(4)
-    spread(1)
-    for w in weights:
-        w.wait()
-    if tight:
-        expert(0)
-    relay(5)
-    relay(6)
-    spread(2)
-    if tight:
-        expert(1)
-        combine(0)
-    relay(7)
-    relay(8)
-    relay(9)
-    spread(3)
-
-    def early(d, hop, rel):
-        if rel or hop > 6:
-            return None
-        if hop == 6:
-            return off[d] == SPAN - 1
-        return off[d] >= SPAN - 2
-
-    def hand_back(hop, when):
-        for rel in reversed(kinds_at(hop)):
-            for unit in (0, 1):
-                for d in (0, 1):
-                    fine = valid(off[d], hop, rel)
-                    if unit == 1 and rel == 0:
-                        fine = fine & (off[d] < SPAN - 1)
-                    ahead = early(d, hop, rel)
-                    if when == "end":
-                        if ahead is None or unit == 1:
-                            continue
-                        fine = fine & (off[d] == SPAN - 1)
-                    elif when == "middle":
-                        if ahead is None or hop == 6:
-                            continue
-                        fine = fine & (off[d] == SPAN - 2)
-                    elif when == "rest" and ahead is not None:
-                        fine = fine & jnp.logical_not(ahead)
-                    index = first_block(hop) + rel
-                    b, k = where_part(d, hop) if rel == 0 else (0, 0)
-
-                    @pl.when(fine)
-                    def _():
-                        if rel == 0:
-                            if hop < HOPS and when != "end":
-                                later = first_block(hop + 1)
-
-                                @pl.when(off[d] < SPAN - 1 - unit)
-                                def _():
-                                    backward(d, back.at[d, later, pieces[unit]], later, unit).wait_recv()
-                                    part[b, k, pieces[unit]] = (
-                                        part[b, k, pieces[unit]].astype(F32) + back[d, later, pieces[unit]].astype(F32)
-                                    ).astype(BF16)
-
-                            backward(d, part.at[b, k, pieces[unit]], index, unit).start()
-                        else:
-                            later = first_block(hop + 1) + rel - last[d]
-                            backward(d, back.at[d, later, pieces[unit]], later, unit).wait_recv()
-                            backward(d, back.at[d, later, pieces[unit]], index, unit).start()
-
-    if tight:
-        expert(2)
-        combine(1)
-        combine(2)
-        for hop in range(6, 0, -1):
-            hand_back(hop, "end")
-        expert(3)
-        for hop in range(5, 0, -1):
-            hand_back(hop, "middle")
+    acts = dict(r=relay, s=spread, e=expert, c=combine, w=item)
+    if cap < WIDE:
+        fresh = True
+        for name, *where in ORDER:
+            if name == "e" and fresh:
+                for w in weights:
+                    w.wait()
+                fresh = False
+            acts[name](*where)
     else:
-
-        @pl.loop(0, len(batches))
-        def _(b):
-            expert(b)
-
-        for b in range(len(batches) - 1):
-            combine(b)
-    combine(3)
-    for hop in range(HOPS, 0, -1):
-        hand_back(hop, "rest" if tight else "all")
+        for hop in range(1, HOPS + 1):
+            relay(hop)
+        for w in weights:
+            w.wait()
+        for act in (spread, expert, combine):
+
+            @pl.loop(0, 6)
+            def _(b):
+                act(b)
+
+            act(6)
+            act(7)
+        for hop in range(HOPS, 0, -1):
+            for end in range(hop, HOPS + 1):
+                if real(end - hop, end):
+                    item(end - hop, end)
 
     first_hop(lambda copy, d, rel, unit: backward(d, back.at[d, rel, pieces[unit]], rel, unit).wait_recv())
     group, up_rank, down_rank = r["gc"], r["Pc"], r["Mc"]
@@ -420,14 +427,19 @@
         (group == lax.rem(g0 + 1, GROUPS), up_rank, back.at[0, 1 - last[0]]),
         (group == lax.rem(g0 + GROUPS - 1, GROUPS), down_rank, back.at[1, 1 - last[1]]),
         (group == lax.rem(g0 + 2, GROUPS), far_rank, back.at[far, 2 - jnp.where(zo >= 2, last[0], last[1])]),
-        (group == g0, up_rank, part.at[3, 0]),
+        (group == g0, up_rank, part.at[6, 0]),
     ]
     lanes = iota((tokens, len(plan) * cap), 1)
     pick = jnp.zeros(lanes.shape, F32)
     for i, (mask, rank, _) in enumerate(plan):
         pick = pick + jnp.where(jnp.where(mask, rank + i * cap, -1) == lanes, 1.0, 0.0)
-    blocks = jnp.concatenate([ref[...] for _, _, ref in plan], axis=0)
-    out_ref[...] = jnp.dot(pick.astype(BF16), blocks, preferred_element_type=F32)
+    pick = pick.astype(BF16)
+
+    @pl.loop(0, out_ref.shape[1] // 512)
+    def _(i):
+        cols = pl.ds(pl.multiple_of(i * 512, 512), 512)
+        blocks = jnp.concatenate([ref[:, cols] for _, _, ref in plan], axis=0)
+        out_ref[:, cols] = jnp.dot(pick, blocks, preferred_element_type=F32)
 
     first_hop(lambda copy, *_: copy.wait_send())
     for hop in range(1, HOPS + 1):
@@ -443,7 +455,7 @@
             backward(d, back.at[d, index, pieces[unit]], index, unit).wait_send()
 
         arrivals(hop, done)
-    for b in range(len(batches)):
+    for b in range(BATCHES):
         for k in range(1, SEATS):
             spread_copy(b, k).wait_send()
             return_copy(b, k).wait_send()
@@ -453,7 +465,7 @@
     rows, width = normed.shape
     inner = w_gate.shape[2]
     far = pl.BlockSpec(memory_space=pltpu.HBM)
-    seats = pltpu.VMEM((4, SEATS, 16, width), BF16)
+    seats = pltpu.VMEM((BATCHES, SEATS, 8, width), BF16)
     dma = pltpu.SemaphoreType.DMA
     return pl.pallas_call(
         functools.partial(moe_body, cap),
@@ -467,14 +479,15 @@
             pltpu.VMEM((width, inner), BF16),
             pltpu.VMEM((width, inner), BF16),
             pltpu.VMEM((inner, width), BF16),
+            pltpu.VMEM((SEATS * 8, inner), BF16),
             pltpu.VMEM((2, GROUPS, cap, width), BF16),
             pltpu.VMEM((2, BLOCKS, cap, width), BF16),
             pltpu.VMEM((2, BLOCKS, cap, width), BF16),
-            pltpu.VMEM((4, 4, cap, width), BF16),
+            pltpu.VMEM((BATCHES, 2, cap, width), BF16),
             seats, seats, seats, seats,
             dma((3,)), dma((3,)),
             dma((2, BLOCKS, 2)), dma((2, BLOCKS, 2)), dma((2, BLOCKS, 2)), dma((2, BLOCKS, 2)),
-            dma((4, SEATS)), dma((4,)), dma((4, SEATS)), dma((4,)),
+            dma((BATCHES, SEATS)), dma((BATCHES,)), dma((BATCHES, SEATS)), dma((BATCHES,)),
         ],
         compiler_params=pltpu.CompilerParams(
             collective_id=1 if cap == WIDE else 3, has_side_effects=True, vmem_limit_bytes=60 << 20

time: 203 us -> 180 us (0.89)
  Pallas kernels: 200 us -> 176 us
    pallas_call x1, Pallas kernels: 154 us -> 130 us  [experts_kernel(): pl.pallas_call(functools.partial(moe_body, cap), out_shape=jax.ShapeDtype...]
where the time goes in v4:
time: 180 us; the launch traced here: 179 us
  Pallas kernels  176 us (98%)
  other arithmetic  1.94 us (1%)
    pallas_call x1, Pallas kernels, experts_kernel(): pl.pallas_call(functools.partial(moe_body, cap), out_shape=jax.ShapeDtype...  130 us
    pallas_call x1, Pallas kernels, front_kernel(): pl.pallas_call(front_body, out_shape=(jax.ShapeDtypeStruct((rows, width),...  46.1 us

profile of v4, /device:TPU:40, one launch (start us, length us, event | category | flops | bytes accessed | tf_op | source)
XLA Modules:
  0.0 179.2 jit_solution(9178779064334427210)
XLA Ops:
  0.0 0.0 copy-start
  0.0 0.0 copy-start.1
  0.0 46.1 %shard_map.145 = (bf16[128,2048]{1,0:T(8,128)(2,1)}, bf16[128,2048]{1,0:T(8,128)(2,1)S(1)}, f32[16,8,128]{2,1,0:T(8,128)S(1)}, s32[1]{0:T(128)}) custom-call(bf16[512,256]{1,0:T(8,128)(2,1)} %value_hbm.1, bf16[512,256]{1,0:T(8,128)(2,1)} %gate_hbm.1, bf16[31,256]{1,0:T(8,128)(2,1)} %taps_hbm.1, f32[1,256]{1,0:T(1,128)} %bitcast.12, f32[1,256]{1,0:T(1,128)} %bitcast.13, ...), custom_call_target="tpu_custom_call" | custom-call | tf_op jit(solution)/shard_map/pallas_call | solution.py:767
  46.8 0.0 copy-done
  46.8 0.0 copy-done.1
  46.8 130.4 %conditional.1 = (f32[128,2048]{1,0:T(8,128)S(1)}) conditional(s32[]{:T(128)} %bitcast.7, (bf16[128,2048]{1,0:T(8,128)(2,1)S(1)}, s32[2,128]{1,0:T(2,128)S(1)}, f32[16,8,128]{2,1,0:T(8,128)S(1)}, bf16[1,2048,512]{2,1,0:T(8,128)(2,1)S(1)}, bf16[1,2048,512]{2,1,0:T(8,128)(2,1)}, /*index=5*/bf16[1,512,2048]{2,1,0:T(8,128)(2,1)}) %tuple.16, ...), branch_computations={%region_0.0_spmd, %region_1.0_spmd} | conditional | bytes 8 | solution.py:826
  46.8 130.1 %branch_0_fun.1 = f32[128,2048]{1,0:T(8,128)S(1)} custom-call(bf16[128,2048]{1,0:T(8,128)(2,1)S(1)} %get-tuple-element.32.normed_hbm, s32[2,128]{1,0:T(2,128)S(1)} %get-tuple-element.33.row_hbm, f32[16,8,128]{2,1,0:T(8,128)S(1)} %get-tuple-element.34.meta_hbm, bf16[1,2048,512]{2,1,0:T(8,128)(2,1)S(1)} %get-tuple-element.35.wg_hbm, ...), custom_call_target="tpu_custom_call" | custom-call | tf_op jit(solution)/shard_map/cond/branch_0_fun/pallas_call | solution.py:470
  177.2 1.9 %add_convert_fusion = bf16[128,2048]{1,0:T(8,128)(2,1)} fusion(f32[128,2048]{1,0:T(8,128)S(1)} %get-tuple-element.52, bf16[128,2048]{1,0:T(8,128)(2,1)} %get-tuple-element.48), kind=kLoop, calls=%fused_computation | loop fusion | flops 786432 | bytes 2097152 | tf_op jit(solution)/shard_map/convert_element_type | solution.py:832
Async XLA Ops:
  0.0 46.8 %copy-start = (bf16[1,2048,512]{2,1,0:T(8,128)(2,1)S(1)}, bf16[1,2048,512]{2,1,0:T(8,128)(2,1)}, u32[]{:S(2)}) copy-start(bf16[1,2048,512]{2,1,0:T(8,128)(2,1)} %param.29) | copy-start | bytes 6291460
  0.0 46.8 %copy-start.1 = (s32[128,2]{0,1:T(2,128)S(1)}, s32[128,2]{0,1:T(2,128)}, u32[]{:S(2)}) copy-start(s32[128,2]{0,1:T(2,128)} %param.27) | copy-start | bytes 3076

commit v5 on v4

--- a/solution.py
+++ b/solution.py
@@ -103,14 +103,13 @@
     return out
 
 
-def route_tables(row, loads, meta_ref, zed):
+def route_tables(r, row, cols, meta_ref, zed):
     size = row.shape[1]
-    cols = columns_of(row, loads)
     col = cols[:, 0:2].astype(jnp.int32)
     zo, g0 = lax.rem(zed, SPAN), lax.div(zed, SPAN)
-    r = ranks(col, row)
     e1c, e2c = col[:, 0:1], col[:, 1:2]
     e1r, e2r = row[0:1, :], row[1:2, :]
+    crowd = jnp.where(r["Pr"] >= NARROW, 1.0, 0.0)
     earlier = r["lane"] < r["sub"]
     place = []
     for e in (e1c, e2c):
@@ -133,8 +132,7 @@
             hit = lane == lanes
             slot_row = slot_row + jnp.sum(jnp.where(hit, slot + 1.0, 0.0), axis=0, keepdims=True)
             weight_row = weight_row + jnp.sum(jnp.where(hit, cols[:, 2 + k : 3 + k], 0.0), axis=0, keepdims=True)
-        meta_ref[plane] = jnp.concatenate([slot_row, weight_row, jnp.zeros((6, 128), F32)], axis=0)
-    return jnp.broadcast_to(jnp.where(r["Pr"] >= NARROW, 1.0, 0.0), (8, size))
+        meta_ref[plane] = jnp.concatenate([slot_row, weight_row, crowd, jnp.zeros((5, 128), F32)], axis=0)
 
 
 def columns_of(*rows):
@@ -143,11 +141,10 @@
     return jnp.transpose(stack, (1, 0))
 
 
-def moe_body(
-    cap, normed_hbm, row_hbm, meta_hbm, wg_hbm, wu_hbm, wd_hbm, out_ref,
-    normed_ref, row_ref, meta_ref, wg, wu, wd, active, own, came, back, part, xs, xr, rb, yr,
-    isem, wsem, fsend, frecv, bsend, brecv, xsend, xrecv, ysend, yrecv,
-):
+def routing(cap, base, r, normed_ref, meta_ref, wg_hbm, wu_hbm, wd_hbm, out_ref, work):
+    (wg, wu, wd, active, own, came, back, part, xs, xr, rb, yr,
+     wsem, fsend, frecv, bsend, brecv, xsend, xrecv, ysend, yrecv) = work
+    tokens = normed_ref.shape[0]
     sp, tp = lax.axis_index("sp"), lax.axis_index("tp")
     zed, core = lax.div(sp, 2), lax.rem(sp, 2)
     zo, g0 = lax.rem(zed, SPAN), lax.div(zed, SPAN)
@@ -161,44 +158,28 @@
     def seat_device(s):
         return {"sp": zed * 2 + lax.div(s, 4), "tp": lax.rem(s, 4)}
 
-    small = [
-        pltpu.make_async_copy(row_hbm, row_ref, isem.at[0]),
-        pltpu.make_async_copy(normed_hbm, normed_ref, isem.at[1]),
-        pltpu.make_async_copy(meta_hbm, meta_ref, isem.at[2]),
-    ]
-    for w in small:
-        w.start()
-    pieces = (pl.ds(0, UNIT), pl.ds(UNIT, cap - UNIT))
+    pieces = (pl.ds(0, UNIT), pl.ds(UNIT, cap - UNIT)) if cap > UNIT else (pl.ds(0, cap),)
+    units = range(len(pieces))
     weights = [
         pltpu.make_async_copy(wg_hbm.at[0], wg, wsem.at[0]),
         pltpu.make_async_copy(wu_hbm.at[0], wu, wsem.at[1]),
         pltpu.make_async_copy(wd_hbm.at[0], wd, wsem.at[2]),
     ]
-    for w in weights:
-        w.start()
-
-    for d in (0, 1):
-        for i in range(3):
-            back[d, i] = jnp.zeros(back.shape[2:], BF16)
-
-        @pl.when(off[d] == SPAN - 1)
-        def _():
-            for hop in range(1, HOPS + 1):
-                came[d, first_block(hop), UNIT:cap] = jnp.zeros((cap - UNIT, came.shape[3]), BF16)
-
-    barrier = pltpu.get_barrier_semaphore()
-    for to in ring_to:
-        pl.semaphore_signal(barrier, inc=1, device_id=to, device_id_type=MESH)
-    for k in range(1, SEATS):
-        pl.semaphore_signal(barrier, inc=1, device_id=seat_device(lax.rem(seat + k, SEATS)), device_id_type=MESH)
-
-    small[0].wait()
-    row = row_ref[...]
-    tokens = row.shape[1]
-    r = ranks(columns_of(row)[:, 0:2].astype(jnp.int32), row)
-    small[1].wait()
-    for d, name in ((0, "P"), (1, "M")):
-        slot = r["gr"] * cap + r[name + "r"]
+    def prepare():
+        for w in weights:
+            w.start()
+        for d in (0, 1):
+            for i in range(3):
+                back[d, i] = jnp.zeros(back.shape[2:], BF16)
+            if cap > UNIT:
+
+                @pl.when(off[d] == SPAN - 1)
+                def _():
+                    for hop in range(1, HOPS + 1):
+                        came[d, first_block(hop), UNIT:cap] = jnp.zeros((cap - UNIT, came.shape[3]), BF16)
+
+    def pack_own(d, name):
+        slot = jnp.where((r[name + "r"] >= base) & (r[name + "r"] < base + cap), r["gr"] * cap + r[name + "r"] - base, -1)
         onehot = jnp.where(iota((GROUPS * cap, tokens), 0) == slot, 1.0, 0.0).astype(BF16)
 
         @pl.loop(0, own.shape[-1] // 512)
@@ -207,8 +188,6 @@
             rows = jnp.dot(onehot, normed_ref[:, cols], preferred_element_type=F32).astype(BF16)
             own[d, :, :, cols] = rows.reshape(GROUPS, cap, 512)
 
-    pl.semaphore_wait(barrier, SEATS + 1)
-
     def forward(d, src, hop, index, unit):
         return pltpu.make_async_remote_copy(
             src_ref=src, dst_ref=came.at[d, index, pieces[unit]],
@@ -225,7 +204,7 @@
 
     def first_hop(act):
         for rel in kinds_at(1):
-            for unit in (0, 1):
+            for unit in units:
                 for d in (0, 1):
                     kind = rel + last[d]
                     group = lax.rem(g0 + kind, GROUPS) if d == 0 else lax.rem(g0 + GROUPS - kind, GROUPS)
@@ -237,11 +216,9 @@
                     def _():
                         act(forward(d, own.at[d, group, pieces[unit]], 1, rel, unit), d, rel, unit)
 
-    first_hop(lambda copy, *_: copy.start())
-
     def arrivals(hop, act):
         for rel in kinds_at(hop):
-            for unit in (0, 1):
+            for unit in units:
                 for d in (0, 1):
                     fine = valid(off[d], hop, rel)
                     if unit == 1 and rel == 0:
@@ -297,7 +274,7 @@
             meta = meta_ref[whose]
             if k:
                 meta = pltpu.roll(meta, 4 * k, 1)
-            slots.append(iota((cap, SEATS * 8), 0).astype(F32) == meta[0:1, 0 : SEATS * 8])
+            slots.append((iota((cap, SEATS * 8), 0) + base).astype(F32) == meta[0:1, 0 : SEATS * 8])
             loads.append(meta[1:2, 0 : SEATS * 8])
         return slots, loads
 
@@ -374,7 +351,7 @@
             @pl.when(off[d] == place)
             def _():
                 index = first_block(hop) + rel
-                for unit in (0, 1):
+                for unit in units:
                     if rel:
                         later = first_block(hop + 1) + rel - (place == SPAN - 1)
                         backward(d, back.at[d, later, pieces[unit]], later, unit).wait_recv()
@@ -389,17 +366,24 @@
                             mine[...] = (mine[...].astype(F32) + far[...].astype(F32)).astype(BF16)
                         backward(d, mine, index, unit).start()
 
-    small[2].wait()
     acts = dict(r=relay, s=spread, e=expert, c=combine, w=item)
-    if cap < WIDE:
-        fresh = True
-        for name, *where in ORDER:
-            if name == "e" and fresh:
-                for w in weights:
-                    w.wait()
-                fresh = False
-            acts[name](*where)
-    else:
+
+    def send_own():
+        pack_own(0, "P")
+        pack_own(1, "M")
+        first_hop(lambda copy, *_: copy.start())
+
+    def trip(pause):
+        if cap == NARROW:
+            fresh = True
+            for name, *where in ORDER:
+                if name == "e" and fresh:
+                    for w in weights:
+                        w.wait()
+                    pause()
+                    fresh = False
+                acts[name](*where)
+            return
         for hop in range(1, HOPS + 1):
             relay(hop)
         for w in weights:
@@ -417,91 +401,131 @@
                 if real(end - hop, end):
                     item(end - hop, end)
 
-    first_hop(lambda copy, d, rel, unit: backward(d, back.at[d, rel, pieces[unit]], rel, unit).wait_recv())
-    group, up_rank, down_rank = r["gc"], r["Pc"], r["Mc"]
-    far = jnp.where(zo >= 2, 0, 1)
-    far_rank = jnp.where(zo >= 2, up_rank, down_rank)
-    plan = [
-        ((group == g0) & (r["mxc"] > zo), up_rank, back.at[0, 0]),
-        ((group == g0) & (r["mnc"] < zo), down_rank, back.at[1, 0]),
-        (group == lax.rem(g0 + 1, GROUPS), up_rank, back.at[0, 1 - last[0]]),
-        (group == lax.rem(g0 + GROUPS - 1, GROUPS), down_rank, back.at[1, 1 - last[1]]),
-        (group == lax.rem(g0 + 2, GROUPS), far_rank, back.at[far, 2 - jnp.where(zo >= 2, last[0], last[1])]),
-        (group == g0, up_rank, part.at[6, 0]),
+    def home():
+        first_hop(lambda copy, d, rel, unit: backward(d, back.at[d, rel, pieces[unit]], rel, unit).wait_recv())
+        group, up_rank, down_rank = r["gc"], r["Pc"], r["Mc"]
+        far = jnp.where(zo >= 2, 0, 1)
+        far_rank = jnp.where(zo >= 2, up_rank, down_rank)
+        plan = [
+            ((group == g0) & (r["mxc"] > zo), up_rank, back.at[0, 0]),
+            ((group == g0) & (r["mnc"] < zo), down_rank, back.at[1, 0]),
+            (group == lax.rem(g0 + 1, GROUPS), up_rank, back.at[0, 1 - last[0]]),
+            (group == lax.rem(g0 + GROUPS - 1, GROUPS), down_rank, back.at[1, 1 - last[1]]),
+            (group == lax.rem(g0 + 2, GROUPS), far_rank, back.at[far, 2 - jnp.where(zo >= 2, last[0], last[1])]),
+            (group == g0, up_rank, part.at[6, 0]),
+        ]
+        lanes = iota((tokens, len(plan) * cap), 1)
+        pick = jnp.zeros(lanes.shape, F32)
+        for i, (mask, rank, _) in enumerate(plan):
+            pick = pick + jnp.where(jnp.where(mask & (rank >= base) & (rank < base + cap), rank - base + i * cap, -1) == lanes, 1.0, 0.0)
+        pick = pick.astype(BF16)
+
+        @pl.loop(0, out_ref.shape[1] // 512)
+        def _(i):
+            cols = pl.ds(pl.multiple_of(i * 512, 512), 512)
+            blocks = jnp.concatenate([ref[:, cols] for _, _, ref in plan], axis=0)
+            out_ref[:, cols] = jnp.dot(pick, blocks, preferred_element_type=F32)
+
+    def settle():
+        first_hop(lambda copy, *_: copy.wait_send())
+        for hop in range(1, HOPS + 1):
+            def done(d, rel, unit):
+                index = first_block(hop) + rel
+                if hop < HOPS:
+                    ok, there = goes_on(d, hop, rel, unit)
+
+                    @pl.when(ok)
+                    def _():
+                        forward(d, came.at[d, index, pieces[unit]], hop + 1, there, unit).wait_send()
+
+                backward(d, back.at[d, index, pieces[unit]], index, unit).wait_send()
+
+            arrivals(hop, done)
+        for b in range(BATCHES):
+            for k in range(1, SEATS):
+                spread_copy(b, k).wait_send()
+                return_copy(b, k).wait_send()
+
+    return prepare, send_own, trip, home, settle
+
+
+def rest_body(normed_hbm, row_hbm, meta_hbm, wg_hbm, wu_hbm, wd_hbm, out_ref, normed_ref, row_ref, meta_ref, isem, *work):
+    small = [
+        pltpu.make_async_copy(row_hbm, row_ref, isem.at[0]),
+        pltpu.make_async_copy(normed_hbm, normed_ref, isem.at[1]),
+        pltpu.make_async_copy(meta_hbm, meta_ref, isem.at[2]),
     ]
-    lanes = iota((tokens, len(plan) * cap), 1)
-    pick = jnp.zeros(lanes.shape, F32)
-    for i, (mask, rank, _) in enumerate(plan):
-        pick = pick + jnp.where(jnp.where(mask, rank + i * cap, -1) == lanes, 1.0, 0.0)
-    pick = pick.astype(BF16)
-
-    @pl.loop(0, out_ref.shape[1] // 512)
-    def _(i):
-        cols = pl.ds(pl.multiple_of(i * 512, 512), 512)
-        blocks = jnp.concatenate([ref[:, cols] for _, _, ref in plan], axis=0)
-        out_ref[:, cols] = jnp.dot(pick, blocks, preferred_element_type=F32)
-
-    first_hop(lambda copy, *_: copy.wait_send())
-    for hop in range(1, HOPS + 1):
-        def done(d, rel, unit):
-            index = first_block(hop) + rel
-            if hop < HOPS:
-                ok, there = goes_on(d, hop, rel, unit)
-
-                @pl.when(ok)
-                def _():
-                    forward(d, came.at[d, index, pieces[unit]], hop + 1, there, unit).wait_send()
-
-            backward(d, back.at[d, index, pieces[unit]], index, unit).wait_send()
-
-        arrivals(hop, done)
-    for b in range(BATCHES):
-        for k in range(1, SEATS):
-            spread_copy(b, k).wait_send()
-            return_copy(b, k).wait_send()
-
-
-def experts_kernel(cap, normed, ids, meta, w_gate, w_up, w_down):
-    rows, width = normed.shape
-    inner = w_gate.shape[2]
-    far = pl.BlockSpec(memory_space=pltpu.HBM)
+    for w in small:
+        w.start()
+    for w in small:
+        w.wait()
+    row = row_ref[...]
+    r = ranks(columns_of(row)[:, 0:2].astype(jnp.int32), row)
+    prepare, send_own, trip, home, settle = routing(
+        WIDE - NARROW, NARROW, r, normed_ref, meta_ref, wg_hbm, wu_hbm, wd_hbm, out_ref, work
+    )
+    prepare()
+    sp, tp = lax.axis_index("sp"), lax.axis_index("tp")
+    zed, core = lax.div(sp, 2), lax.rem(sp, 2)
+    teams = lax.axis_size("tp")
+    barrier = pltpu.get_barrier_semaphore()
+    for step in (1, PLANES - 1):
+        to = {"sp": lax.rem(zed + step, PLANES) * 2 + core}
+        pl.semaphore_signal(barrier, inc=1, device_id=to, device_id_type=MESH)
+    for k in range(1, teams):
+        pl.semaphore_signal(barrier, inc=1, device_id={"tp": lax.rem(tp + k, teams)}, device_id_type=MESH)
+    for k in range(teams):
+        pl.semaphore_signal(barrier, inc=1, device_id={"sp": zed * 2 + 1 - core, "tp": k}, device_id_type=MESH)
+    pl.semaphore_wait(barrier, 2 * teams + 1)
+    send_own()
+    trip(None)
+    home()
+    settle()
+
+
+def work_shapes(cap, width, inner):
     seats = pltpu.VMEM((BATCHES, SEATS, 8, width), BF16)
     dma = pltpu.SemaphoreType.DMA
+    return [
+        pltpu.VMEM((width, inner), BF16),
+        pltpu.VMEM((width, inner), BF16),
+        pltpu.VMEM((inner, width), BF16),
+        pltpu.VMEM((SEATS * 8, inner), BF16),
+        pltpu.VMEM((2, GROUPS, cap, width), BF16),
+        pltpu.VMEM((2, BLOCKS, cap, width), BF16),
+        pltpu.VMEM((2, BLOCKS, cap, width), BF16),
+        pltpu.VMEM((BATCHES, 2, cap, width), BF16),
+        seats, seats, seats, seats,
+        dma((3,)),
+        dma((2, BLOCKS, 2)), dma((2, BLOCKS, 2)), dma((2, BLOCKS, 2)), dma((2, BLOCKS, 2)),
+        dma((BATCHES, SEATS)), dma((BATCHES,)), dma((BATCHES, SEATS)), dma((BATCHES,)),
+    ]
+
+
+def rest_kernel(normed, ids, meta, w_gate, w_up, w_down):
+    rows, width = normed.shape
     return pl.pallas_call(
-        functools.partial(moe_body, cap),
+        rest_body,
         out_shape=jax.ShapeDtypeStruct((rows, width), F32),
-        in_specs=[far] * 6,
+        in_specs=[pl.BlockSpec(memory_space=pltpu.HBM)] * 6,
         out_specs=pl.BlockSpec(memory_space=pltpu.VMEM),
         scratch_shapes=[
             pltpu.VMEM((rows, width), BF16),
             pltpu.VMEM(ids.shape, jnp.int32),
             pltpu.VMEM(meta.shape, F32),
-            pltpu.VMEM((width, inner), BF16),
-            pltpu.VMEM((width, inner), BF16),
-            pltpu.VMEM((inner, width), BF16),
-            pltpu.VMEM((SEATS * 8, inner), BF16),
-            pltpu.VMEM((2, GROUPS, cap, width), BF16),
-            pltpu.VMEM((2, BLOCKS, cap, width), BF16),
-            pltpu.VMEM((2, BLOCKS, cap, width), BF16),
-            pltpu.VMEM((BATCHES, 2, cap, width), BF16),
-            seats, seats, seats, seats,
-            dma((3,)), dma((3,)),
-            dma((2, BLOCKS, 2)), dma((2, BLOCKS, 2)), dma((2, BLOCKS, 2)), dma((2, BLOCKS, 2)),
-            dma((BATCHES, SEATS)), dma((BATCHES,)), dma((BATCHES, SEATS)), dma((BATCHES,)),
-        ],
-        compiler_params=pltpu.CompilerParams(
-            collective_id=1 if cap == WIDE else 3, has_side_effects=True, vmem_limit_bytes=60 << 20
-        ),
+            pltpu.SemaphoreType.DMA((3,)),
+        ] + work_shapes(WIDE - NARROW, width, w_gate.shape[2]),
+        compiler_params=pltpu.CompilerParams(collective_id=1, has_side_effects=True, vmem_limit_bytes=60 << 20),
     )(normed, ids, meta, w_gate, w_up, w_down)
 
 
-def front_body(
+def main_body(
     value_hbm, gate_hbm, taps_hbm, bias_hbm, scale_hbm, shift_hbm, branch_hbm, gain_hbm, row_hbm, load_hbm,
-    weight_hbm, residual_hbm,
-    hidden_ref, normed_ref, meta_ref, crowd_ref,
-    value_ref, gate_ref, taps_ref, vectors, gain_ref, row_ref, load_ref, weight, residual, gated, grown, packs, conv,
+    weight_hbm, residual_hbm, wg_hbm, wu_hbm, wd_hbm,
+    hidden_hbm, normed_hbm, meta_hbm, out_ref, crowd_ref,
+    hidden_ref, normed_ref, meta_ref, value_ref, gate_ref, taps_ref, vectors, gain_ref, row_ref, load_ref, weight, residual, gated, grown, packs, conv,
     tables, flags, heard,
-    lsem, csend, crecv, gsend, grecv, hsend, hrecv, psend, precv, tsend, trecv,
+    lsem, osem, csend, crecv, gsend, grecv, hsend, hrecv, psend, precv, tsend, trecv, *work,
 ):
     sp, tp = lax.axis_index("sp"), lax.axis_index("tp")
     steps, teams = lax.axis_size("sp"), lax.axis_size("tp")
@@ -547,11 +571,7 @@
     for k in range(1, parts):
         pl.semaphore_signal(barrier, inc=1, device_id={"grp": part_of(k)}, device_id_type=MESH)
 
-    for copy in fetch:
-        copy.wait()
-    crowd = route_tables(row_ref[...], load_ref[...], tables, zed)
-    flags[0] = crowd
-    for copy in first:
+    for copy in fetch + first:
         copy.wait()
     passed = (value_ref[...].astype(F32) * jax.nn.sigmoid(gate_ref[...].astype(F32))).astype(BF16)
     gated[...] = passed.reshape(gated.shape)
@@ -563,6 +583,13 @@
     def _():
         grown[:, 0] = jnp.zeros((teams, UNIT, channels), BF16)
 
+    row = row_ref[...]
+    cols = columns_of(row, load_ref[...])
+    r = ranks(cols[:, 0:2].astype(jnp.int32), row)
+    prepare, send_own, trip, home, settle = routing(
+        NARROW, 0, r, normed_ref, meta_ref, wg_hbm, wu_hbm, wd_hbm, out_ref, work
+    )
+    prepare()
     pl.semaphore_wait(barrier, 2 * teams + PLANES + parts - 3 + jnp.where(sp < steps - 1, 1, 0))
 
     def whole(to, k):
@@ -599,12 +626,9 @@
 
     def table_copy(k):
         return pltpu.make_async_remote_copy(
-            src_ref=tables.at[column(k)  // 2], dst_ref=meta_land(k), send_sem=tsend.at[k], recv_sem=trecv.at[k],
-            device_id={"sp": column(k)}, device_id_type=MESH,
-        )
-
-    def meta_land(k):
-        return tables.at[PLANES + k]
+            src_ref=tables.at[lax.rem(zed + k, PLANES)], dst_ref=meta_ref.at[zed], send_sem=tsend.at[k],
+            recv_sem=trecv.at[k], device_id={"sp": column(k)}, device_id_type=MESH,
+        )
 
     for k in (2, 1, 3):
         pack_copy(k).start()
@@ -618,47 +642,30 @@
     def _():
         halo(tp).start()
 
-    for k in range(1, PLANES):
-        table_copy(k).start()
-
-    plane_mates = [{"tp": team(k)} for k in range(1, teams)] + [{"sp": other, "tp": k} for k in range(teams)]
-    rounds = [
-        [(to, i) for i, to in enumerate(plane_mates)],
-        [({"grp": part_of(k)}, k) for k in range(1, parts)],
-        [({"sp": column(k)}, k) for k in range(1, PLANES)],
-    ]
+    mates = [{"tp": team(k)} for k in range(1, teams)] + [{"sp": other, "tp": k} for k in range(teams)]
+    peers = [{"grp": part_of(k)} for k in range(1, parts)]
 
     def flag_copies(stage):
-        base = (0, 16, 16 + parts)[stage]
-        return [
+        out = []
+        for i, to in enumerate(peers if stage else mates):
+            at = i + SEATS * stage
+            land = teams - 1 + tp if not stage and i >= teams - 1 else at
+            out.append(pltpu.make_async_remote_copy(
+                src_ref=flags.at[stage], dst_ref=heard.at[land], send_sem=csend.at[at],
+                recv_sem=crecv.at[land], device_id=to, device_id_type=MESH,
+            ))
+        return out
+
+    def hear(stage):
+        seen = flags[stage]
+        for i, to in enumerate(peers if stage else mates):
+            at = i + SEATS * stage
             pltpu.make_async_remote_copy(
-                src_ref=flags.at[stage], dst_ref=heard.at[land(stage, base, i)], send_sem=csend.at[base + i],
-                recv_sem=crecv.at[land(stage, base, i)], device_id=to, device_id_type=MESH,
-            )
-            for to, i in rounds[stage]
-        ]
-
-    def land(stage, base, i):
-        if stage == 0 and i >= teams - 1:
-            return base + teams - 1 + tp
-        return base + i
-
-    def hear(stage):
-        base = (0, 16, 16 + parts)[stage]
-        seen = flags[stage]
-        for (to, i) in rounds[stage]:
-            pltpu.make_async_remote_copy(
-                src_ref=flags.at[stage], dst_ref=heard.at[base + i], send_sem=csend.at[base + i],
-                recv_sem=crecv.at[base + i], device_id=to, device_id_type=MESH,
+                src_ref=flags.at[stage], dst_ref=heard.at[at], send_sem=csend.at[at],
+                recv_sem=crecv.at[at], device_id=to, device_id_type=MESH,
             ).wait_recv()
-            seen = jnp.maximum(seen, heard[base + i])
+            seen = jnp.maximum(seen, heard[at])
         flags[stage + 1] = seen
-        if stage < 2:
-            for copy in flag_copies(stage + 1):
-                copy.start()
-
-    for copy in flag_copies(0):
-        copy.start()
 
     for test, size in ((tp == 0, 0), (tp > 0, 1)):
 
@@ -667,6 +674,11 @@
             low = jnp.maximum(tp * pieces - 1, 0) if size else 0
             grown[tp, 1 - size : pieces + 1] = gated[pl.ds(low, pieces + size)]
 
+    route_tables(r, row, cols, tables, zed)
+    meta_ref[zed] = tables[zed]
+    for k in range(1, PLANES):
+        table_copy(k).start()
+
     def wait_part(k):
         source = team(k)
         if k:
@@ -689,8 +701,6 @@
     shift0 = UNIT - reach
     for k in (0, 1, 3, 2):
         wait_part(k)
-        if k in (1, 2):
-            hear(0 if k == 1 else 1)
         source = team(k)
         for half in range(channels // 128):
             lanes = pl.ds(half * 128, 128)
@@ -729,14 +739,36 @@
     scale = lax.rsqrt(jnp.mean(wide * wide, axis=1, keepdims=True) + EPSILON)
     normed_ref[...] = (wide * scale * gain_ref[...]).astype(BF16)
 
-    meta_ref[zed] = tables[zed]
+    send_own()
+    results = [
+        pltpu.make_async_copy(hidden_ref, hidden_hbm, osem.at[0]),
+        pltpu.make_async_copy(normed_ref, normed_hbm, osem.at[1]),
+        pltpu.make_async_copy(meta_ref, meta_hbm, osem.at[2]),
+    ]
     for k in range(1, PLANES):
         table_copy(k).wait_recv()
-        meta_ref[lax.rem(zed + PLANES - k, PLANES)] = tables[PLANES + k]
-
-    hear(2)
-    crowd_ref[0] = jnp.max(flags[3]).astype(jnp.int32)
-    for stage in range(3):
+    for copy in results:
+        copy.start()
+    crowd = meta_ref[0]
+    for z in range(1, PLANES):
+        crowd = jnp.maximum(crowd, meta_ref[z])
+    flags[0] = jnp.broadcast_to(crowd[2:3], crowd.shape)
+    for copy in flag_copies(0):
+        copy.start()
+
+    def pause():
+        hear(0)
+        for copy in flag_copies(1):
+            copy.start()
+
+    trip(pause)
+    hear(1)
+    crowd_ref[0] = jnp.max(flags[2]).astype(jnp.int32)
+    home()
+    settle()
+    for copy in results:
+        copy.wait()
+    for stage in (0, 1):
         for copy in flag_copies(stage):
             copy.wait_send()
 
@@ -756,25 +788,28 @@
         table_copy(k).wait_send()
 
 
-def front_kernel(value, gate, taps, vectors, moe_gain, ids, loads, out_weight, residual):
+def main_kernel(value, gate, taps, vectors, moe_gain, ids, loads, out_weight, residual, w_gate, w_up, w_down):
     rows, width = residual.shape
     tok_rows, channels = value.shape
     teams = lax.axis_size("tp")
-    vmem = pl.BlockSpec(memory_space=pltpu.VMEM)
     far = pl.BlockSpec(memory_space=pltpu.HBM)
     dma = pltpu.SemaphoreType.DMA
-    voices = 16 + lax.axis_size("grp") + PLANES
+    voices = SEATS + lax.axis_size("grp")
     return pl.pallas_call(
-        front_body,
+        main_body,
         out_shape=(
             jax.ShapeDtypeStruct((rows, width), BF16),
             jax.ShapeDtypeStruct((rows, width), BF16),
             jax.ShapeDtypeStruct((PLANES, 8, 128), F32),
+            jax.ShapeDtypeStruct((rows, width), F32),
             jax.ShapeDtypeStruct((1,), jnp.int32),
         ),
-        in_specs=[far] * 12,
-        out_specs=[vmem] * 3 + [pl.BlockSpec(memory_space=pltpu.SMEM)],
+        in_specs=[far] * 15,
+        out_specs=[far] * 3 + [pl.BlockSpec(memory_space=pltpu.VMEM), pl.BlockSpec(memory_space=pltpu.SMEM)],
         scratch_shapes=[
+            pltpu.VMEM((rows, width), BF16),
+            pltpu.VMEM((rows, width), BF16),
+            pltpu.VMEM((PLANES, 8, 128), F32),
             pltpu.VMEM(value.shape, BF16),
             pltpu.VMEM(value.shape, BF16),
             pltpu.VMEM(taps.shape, BF16),
@@ -788,17 +823,17 @@
             pltpu.VMEM((teams, rows // UNIT + 1, UNIT, channels), BF16),
             pltpu.VMEM((teams, 40, channels), F32),
             pltpu.VMEM((teams, rows, channels), F32),
-            pltpu.VMEM((2 * PLANES, 8, 128), F32),
-            pltpu.VMEM((4, 8, 128), F32),
+            pltpu.VMEM((PLANES, 8, 128), F32),
+            pltpu.VMEM((3, 8, 128), F32),
             pltpu.VMEM((voices, 8, 128), F32),
-            dma((12,)), dma((voices,)), dma((voices,)),
+            dma((12,)), dma((3,)), dma((voices,)), dma((voices,)),
             dma((teams,)), dma((teams,)), dma((1,)), dma((teams,)), dma((teams,)), dma((teams,)),
             dma((PLANES,)), dma((PLANES,)),
-        ],
+        ] + work_shapes(NARROW, width, w_gate.shape[2]),
         compiler_params=pltpu.CompilerParams(
             collective_id=2, has_side_effects=True, vmem_limit_bytes=60 << 20
         ),
-    )(value, gate, taps, *vectors, moe_gain, ids, loads, out_weight, residual)
+    )(value, gate, taps, *vectors, moe_gain, ids, loads, out_weight, residual, w_gate, w_up, w_down)
 
 
 def per_device(
@@ -820,16 +855,16 @@
 ):
     ids = expert_ids.T
     vectors = [v[None] for v in (conv_bias, ln_gain, ln_bias, out_gain)]
-    hidden, normed, meta, crowd = front_kernel(
-        conv_value, conv_gate, kernel, vectors, moe_gain[None], ids, expert_weights.T, out_weight, residual
+    hidden, normed, meta, added, crowd = main_kernel(
+        conv_value, conv_gate, kernel, vectors, moe_gain[None], ids, expert_weights.T, out_weight, residual,
+        w_gate, w_up, w_down,
     )
-    added = lax.cond(
+    return lax.cond(
         crowd[0] > 0,
-        functools.partial(experts_kernel, WIDE),
-        functools.partial(experts_kernel, NARROW),
-        normed, ids, meta, w_gate, w_up, w_down,
+        lambda hidden, added, *rest: (hidden.astype(F32) + added + rest_kernel(*rest)).astype(BF16),
+        lambda hidden, added, *_: (hidden.astype(F32) + added).astype(BF16),
+        hidden, added, normed, ids, meta, w_gate, w_up, w_down,
     )
-    return (hidden.astype(F32) + added).astype(BF16)
 
 
 def solution(mesh):

time: 180 us -> 166 us (0.922)
  Pallas kernels: 176 us -> 164 us
    pallas_call x2 -> x1, Pallas kernels: 176 us -> 164 us  [main_kernel(): pl.pallas_call(main_body, out_shape=(jax.ShapeDtypeStruct((rows, width),...]
    convert_element_type x1 -> x0, other arithmetic: 1.94 us -> none  [per_device(): return (hidden.astype(F32) + added).astype(BF16)]
where the time goes in v5:
time: 166 us
  Pallas kernels  164 us (99%)
    pallas_call x1, Pallas kernels, main_kernel(): pl.pallas_call(main_body, out_shape=(jax.ShapeDtypeStruct((rows, width),...  164 us

profile of v5, /device:TPU:40, one launch (start us, length us, event | category | flops | bytes accessed | tf_op | source)
XLA Modules:
  0.0 165.7 jit_solution(3081743123958466018)
XLA Ops:
  0.0 0.0 copy-start
  0.0 0.0 copy-start.1
  0.0 164.2 %shard_map.147 = (bf16[128,2048]{1,0:T(8,128)(2,1)S(1)}, bf16[128,2048]{1,0:T(8,128)(2,1)}, f32[16,8,128]{2,1,0:T(8,128)S(1)}, f32[128,2048]{1,0:T(8,128)S(1)}, s32[1]{0:T(128)}) custom-call(bf16[512,256]{1,0:T(8,128)(2,1)} %value_hbm.1, bf16[512,256]{1,0:T(8,128)(2,1)} %gate_hbm.1, bf16[31,256]{1,0:T(8,128)(2,1)} %taps_hbm.1, f32[1,256]{1,0:T(1,128)} %bitcast.11, ...), custom_call_target="tpu_custom_call" | custom-call | tf_op jit(solution)/shard_map/pallas_call | solution.py:798
  164.8 0.0 copy-done
  164.8 0.0 copy-done.1
  164.8 0.9 conditional.7
  164.8 0.9 convert_add_fusion
Async XLA Ops:
  0.0 164.8 %copy-start = (bf16[1,2048,512]{2,1,0:T(8,128)(2,1)S(1)}, bf16[1,2048,512]{2,1,0:T(8,128)(2,1)}, u32[]{:S(2)}) copy-start(bf16[1,2048,512]{2,1,0:T(8,128)(2,1)} %wg_hbm.1) | copy-start | bytes 6291460
  0.0 164.8 %copy-start.1 = (s32[128,2]{0,1:T(2,128)S(1)}, s32[128,2]{0,1:T(2,128)}, u32[]{:S(2)}) copy-start(s32[128,2]{0,1:T(2,128)} %param.27) | copy-start | bytes 3076

commit v6 on v5

--- a/solution.py
+++ b/solution.py
@@ -202,10 +202,10 @@
             device_id=ring_from[d], device_id_type=MESH,
         )
 
-    def first_hop(act):
+    def first_hop(act, ways=(0, 1)):
         for rel in kinds_at(1):
             for unit in units:
-                for d in (0, 1):
+                for d in ways:
                     kind = rel + last[d]
                     group = lax.rem(g0 + kind, GROUPS) if d == 0 else lax.rem(g0 + GROUPS - kind, GROUPS)
                     fine = valid(following[d], 1, rel)
@@ -369,9 +369,9 @@
     acts = dict(r=relay, s=spread, e=expert, c=combine, w=item)
 
     def send_own():
-        pack_own(0, "P")
-        pack_own(1, "M")
-        first_hop(lambda copy, *_: copy.start())
+        for d in (0, 1):
+            pack_own(d, "PM"[d])
+            first_hop(lambda copy, *_: copy.start(), (d,))
 
     def trip(pause):
         if cap == NARROW:
@@ -868,6 +868,7 @@
 
 
 def solution(mesh):
+    assert mesh.shape["sp"] == 2 * PLANES and 2 * mesh.shape["tp"] == SEATS
     in_specs = (
         P(("grp", "sp"), "tp"),
         P(("grp", "sp"), "tp"),

time: 166 us -> 166 us (level)
  no operation moved by 1% of the time
where the time goes in v6:
time: 166 us
  Pallas kernels  164 us (99%)
    pallas_call x1, Pallas kernels, main_kernel(): pl.pallas_call(main_body, out_shape=(jax.ShapeDtypeStruct((rows, width),...  164 us

profile of v6, /device:TPU:40, one launch (start us, length us, event | category | flops | bytes accessed | tf_op | source)
XLA Modules:
  0.0 165.6 jit_solution(2488422753599268731)
XLA Ops:
  0.0 0.0 copy-start
  0.0 0.0 copy-start.1
  0.0 164.1 %shard_map.147 = (bf16[128,2048]{1,0:T(8,128)(2,1)S(1)}, bf16[128,2048]{1,0:T(8,128)(2,1)}, f32[16,8,128]{2,1,0:T(8,128)S(1)}, f32[128,2048]{1,0:T(8,128)S(1)}, s32[1]{0:T(128)}) custom-call(bf16[512,256]{1,0:T(8,128)(2,1)} %value_hbm.1, bf16[512,256]{1,0:T(8,128)(2,1)} %gate_hbm.1, bf16[31,256]{1,0:T(8,128)(2,1)} %taps_hbm.1, f32[1,256]{1,0:T(1,128)} %bitcast.11, ...), custom_call_target="tpu_custom_call" | custom-call | tf_op jit(solution)/shard_map/pallas_call | solution.py:798
  164.7 0.0 copy-done
  164.7 0.0 copy-done.1
  164.7 0.9 conditional.7
  164.7 0.9 convert_add_fusion
Async XLA Ops:
  0.0 164.7 %copy-start = (bf16[1,2048,512]{2,1,0:T(8,128)(2,1)S(1)}, bf16[1,2048,512]{2,1,0:T(8,128)(2,1)}, u32[]{:S(2)}) copy-start(bf16[1,2048,512]{2,1,0:T(8,128)(2,1)} %wg_hbm.1) | copy-start | bytes 6291460
  0.0 164.7 %copy-start.1 = (s32[128,2]{0,1:T(2,128)S(1)}, s32[128,2]{0,1:T(2,128)}, u32[]{:S(2)}) copy-start(s32[128,2]{0,1:T(2,128)} %param.27) | copy-start | bytes 3076

commit v7 on v6

--- a/solution.py
+++ b/solution.py
@@ -571,10 +571,8 @@
     for k in range(1, parts):
         pl.semaphore_signal(barrier, inc=1, device_id={"grp": part_of(k)}, device_id_type=MESH)
 
-    for copy in fetch + first:
+    for copy in first[2:]:
         copy.wait()
-    passed = (value_ref[...].astype(F32) * jax.nn.sigmoid(gate_ref[...].astype(F32))).astype(BF16)
-    gated[...] = passed.reshape(gated.shape)
     packs[tp, 0 : taps_ref.shape[0]] = taps_ref[...].astype(F32)
     for i in range(4):
         packs[tp, 32 + i : 33 + i] = vectors[i]
@@ -583,9 +581,7 @@
     def _():
         grown[:, 0] = jnp.zeros((teams, UNIT, channels), BF16)
 
-    row = row_ref[...]
-    cols = columns_of(row, load_ref[...])
-    r = ranks(cols[:, 0:2].astype(jnp.int32), row)
+    r = {}
     prepare, send_own, trip, home, settle = routing(
         NARROW, 0, r, normed_ref, meta_ref, wg_hbm, wu_hbm, wd_hbm, out_ref, work
     )
@@ -632,6 +628,11 @@
 
     for k in (2, 1, 3):
         pack_copy(k).start()
+    for copy in first[:2]:
+        copy.wait()
+    passed = (value_ref[...].astype(F32) * jax.nn.sigmoid(gate_ref[...].astype(F32))).astype(BF16)
+    gated[...] = passed.reshape(gated.shape)
+    for k in (2, 1, 3):
         for test, copy in ((team(k) == 0, short), (team(k) > 0, whole)):
 
             @pl.when(test)
@@ -674,6 +675,11 @@
             low = jnp.maximum(tp * pieces - 1, 0) if size else 0
             grown[tp, 1 - size : pieces + 1] = gated[pl.ds(low, pieces + size)]
 
+    for copy in fetch:
+        copy.wait()
+    row = row_ref[...]
+    cols = columns_of(row, load_ref[...])
+    r.update(ranks(cols[:, 0:2].astype(jnp.int32), row))
     route_tables(r, row, cols, tables, zed)
     meta_ref[zed] = tables[zed]
     for k in range(1, PLANES):

time: 166 us -> 166 us (level)
  no operation moved by 1% of the time
where the time goes in v7:
time: 166 us
  Pallas kernels  164 us (99%)
    pallas_call x1, Pallas kernels, main_kernel(): pl.pallas_call(main_body, out_shape=(jax.ShapeDtypeStruct((rows, width),...  164 us

profile of v7, /device:TPU:40, one launch (start us, length us, event | category | flops | bytes accessed | tf_op | source)
XLA Modules:
  0.0 165.8 jit_solution(9839550864662318131)
XLA Ops:
  0.0 0.0 copy-start
  0.0 0.0 copy-start.1
  0.0 164.2 %shard_map.147 = (bf16[128,2048]{1,0:T(8,128)(2,1)S(1)}, bf16[128,2048]{1,0:T(8,128)(2,1)}, f32[16,8,128]{2,1,0:T(8,128)S(1)}, f32[128,2048]{1,0:T(8,128)S(1)}, s32[1]{0:T(128)}) custom-call(bf16[512,256]{1,0:T(8,128)(2,1)} %value_hbm.1, bf16[512,256]{1,0:T(8,128)(2,1)} %gate_hbm.1, bf16[31,256]{1,0:T(8,128)(2,1)} %taps_hbm.1, f32[1,256]{1,0:T(1,128)} %bitcast.11, ...), custom_call_target="tpu_custom_call" | custom-call | tf_op jit(solution)/shard_map/pallas_call | solution.py:804
  164.8 0.0 copy-done
  164.8 0.0 copy-done.1
  164.8 0.9 conditional.7
  164.8 0.9 convert_add_fusion
Async XLA Ops:
  0.0 164.8 %copy-start = (bf16[1,2048,512]{2,1,0:T(8,128)(2,1)S(1)}, bf16[1,2048,512]{2,1,0:T(8,128)(2,1)}, u32[]{:S(2)}) copy-start(bf16[1,2048,512]{2,1,0:T(8,128)(2,1)} %wg_hbm.1) | copy-start | bytes 6291460
  0.0 164.8 %copy-start.1 = (s32[128,2]{0,1:T(2,128)S(1)}, s32[128,2]{0,1:T(2,128)}, u32[]{:S(2)}) copy-start(s32[128,2]{0,1:T(2,128)} %param.27) | copy-start | bytes 3076
